TPU v7x, 512 devices: a whole 4x4x16 slice. The times are simulated.
512 devices in a mesh: ep: 128 (over z, x, core), tp: 4 (over y).
Axes of the slice: x: 4, y: 4, z: 16, core: 2. Of those that a mesh axis runs over, the one named last changes fastest.
Arguments:
- tokens: bfloat16 [6144, 1024], P('ep'), may hold values from -6 to 6
- head_state: float32 [6144, 8, 64, 64], P('ep', 'tp'), may hold values from -6 to 6
- recept_weight: bfloat16 [1024, 512], P(None, 'tp'), may hold values from -0.1875 to 0.1875
- key_weight: bfloat16 [1024, 512], P(None, 'tp'), may hold values from -0.1875 to 0.1875
- value_weight: bfloat16 [1024, 512], P(None, 'tp'), may hold values from -0.1875 to 0.1875
- decay_down_factor: bfloat16 [1024, 64], replicated, may hold values from -0.1875 to 0.1875
- decay_up_factor: bfloat16 [64, 512], P(None, 'tp'), may hold values from -0.75 to 0.75
- decay_base: float32 [512], P('tp'), may hold values from -5 to 3
- rate_down_factor: bfloat16 [1024, 64], replicated, may hold values from -0.1875 to 0.1875
- rate_up_factor: bfloat16 [64, 512], P(None, 'tp'), may hold values from -0.75 to 0.75
- rate_base: float32 [512], P('tp'), may hold values from -3 to 3
- head_gain: float32 [512], P('tp'), may hold values from 0.1 to 1.9
- out_weight: bfloat16 [512, 1024], P('tp'), may hold values from -0.25 to 0.25
- route_experts: int32 [6144, 4], P('ep'), may hold values from 0 to 127, all different within a row; in each aligned block of 48 rows (0 to 47, 48 to 95, ...) at most 3 rows name the same one
- route_weights: float32 [6144, 4], P('ep'), may hold values from 0.03 to 0.2
- expert_gate: bfloat16 [128, 1024, 1024], P('ep', None, 'tp'), may hold values from -1 to 1
- expert_up: bfloat16 [128, 1024, 1024], P('ep', None, 'tp'), may hold values from -1 to 1
- expert_down: bfloat16 [128, 1024, 1024], P('ep', 'tp'), may hold values from -0.1875 to 0.1875
Outputs:
- layer_out: bfloat16 [6144, 1024], P('ep', 'tp')
- new_state: float32 [6144, 8, 64, 64], P('ep', 'tp')
Inputs may be any that keep to these rules, and one draw needn't show every extreme that they name: `route_experts`: each row names 4 different experts. In each aligned block of 48 rows no expert is named by more than 3 rows, a bound that some block reaches.
All inputs are finite; a program needn't handle non-finite values.
Results may differ from a plain program's by a relative error of at most 0.02.
Values may be sent and summed in bfloat16 or wider, within the bound.
A program may use at most 128 MiB of HBM per device.

v0:
```python
import jax
import jax.numpy as jnp
from jax import lax
from jax.sharding import PartitionSpec as P

NORM_EPS = 1e-05
GROUP_EPS = 0.00064
UNIT_EPS = 1e-06
CLAMP_LIMIT = 7.0
GLU_ALPHA = 1.702


def copy_for_each(value, axis):
    length = lax.axis_size(axis)
    return lax.all_to_all(
        jnp.broadcast_to(value[None], (length, *value.shape)), axis, 0, 0, tiled=True
    )


def of_everyone(value, axis):
    return copy_for_each(value, axis).astype(jnp.float32).sum(axis=0)


def laid_out(blocks, dim):
    blocks = jnp.moveaxis(blocks, 0, dim)
    dims = blocks.shape
    return blocks.reshape(*dims[:dim], dims[dim] * dims[dim + 1], *dims[dim + 2 :])


def collect(value, axis, dim):
    return laid_out(copy_for_each(value, axis), dim)


def cut_along(value, dim, length):
    before, after = (value.shape[:dim], value.shape[dim + 1 :])
    return jnp.moveaxis(value.reshape(*before, length, -1, *after), dim, 0)


def sum_at_owner(value, axis, dim):
    length = lax.axis_size(axis)
    blocks = lax.all_to_all(cut_along(value, dim, length), axis, 0, 0, tiled=True)
    return jnp.sum(blocks.astype(jnp.float32), axis=0)


def row_norm(values):
    return values * lax.rsqrt(jnp.mean(values * values, axis=-1, keepdims=True) + NORM_EPS)


def clamped_unit(gate_pre, up_pre):
    gated = jnp.minimum(gate_pre, CLAMP_LIMIT)
    linear = jnp.clip(up_pre, -CLAMP_LIMIT, CLAMP_LIMIT)
    return gated * jax.nn.sigmoid(GLU_ALPHA * gated) * (linear + 1.0)


def update_heads(head_state, recept, keys, values, decay_rate, rate_gate, head_gain):
    seq_count, head_count, head_size = head_state.shape[:3]

    def by_heads(operand):
        return operand.astype(jnp.float32).reshape(seq_count, head_count, head_size)

    recept_heads = by_heads(recept)
    key_heads = by_heads(keys)
    value_heads = by_heads(values)
    decay_heads = by_heads(decay_rate)
    rate_heads = by_heads(rate_gate)
    unit_key = key_heads * lax.rsqrt(
        jnp.sum(key_heads * key_heads, axis=-1, keepdims=True) + UNIT_EPS
    )
    state_unit = jnp.einsum("shvk,shk->shv", head_state, unit_key)
    new_state = (
        head_state * decay_heads[:, :, None, :]
        - state_unit[..., None] * (unit_key * rate_heads)[:, :, None, :]
        + value_heads[..., None] * (key_heads * rate_heads)[:, :, None, :]
    )
    head_out = jnp.einsum("shvk,shk->shv", new_state, recept_heads)
    centre = jnp.mean(head_out, axis=-1, keepdims=True)
    spread = jnp.mean(jnp.square(head_out - centre), axis=-1, keepdims=True)
    normed_heads = (head_out - centre) * lax.rsqrt(spread + GROUP_EPS)
    mixed = (normed_heads.reshape(seq_count, -1) * head_gain).astype(jnp.bfloat16)
    return (new_state, mixed)


def local(
    tokens,
    head_state,
    recept_weight,
    key_weight,
    value_weight,
    decay_down_factor,
    decay_up_factor,
    decay_base,
    rate_down_factor,
    rate_up_factor,
    rate_base,
    head_gain,
    out_weight,
    route_experts,
    route_weights,
    expert_gate,
    expert_up,
    expert_down,
):
    tokens_float = tokens.astype(jnp.float32)
    normed = row_norm(tokens_float).astype(jnp.bfloat16)
    recept = jnp.dot(normed, recept_weight, preferred_element_type=jnp.float32).astype(jnp.bfloat16)
    keys = jnp.dot(normed, key_weight, preferred_element_type=jnp.float32).astype(jnp.bfloat16)
    values = jnp.dot(normed, value_weight, preferred_element_type=jnp.float32).astype(jnp.bfloat16)
    decay_low = jnp.tanh(
        jnp.dot(normed, decay_down_factor, preferred_element_type=jnp.float32)
    ).astype(jnp.bfloat16)
    rate_low = jnp.dot(normed, rate_down_factor, preferred_element_type=jnp.float32).astype(
        jnp.bfloat16
    )
    decay_pre = decay_base + jnp.dot(decay_low, decay_up_factor, preferred_element_type=jnp.float32)
    decay_rate = jnp.exp(-jnp.exp(-jax.nn.softplus(-decay_pre) - 0.5))
    rate_gate = jax.nn.sigmoid(
        rate_base + jnp.dot(rate_low, rate_up_factor, preferred_element_type=jnp.float32)
    )
    new_state, mixed = update_heads(
        head_state, recept, keys, values, decay_rate, rate_gate, head_gain
    )
    partial_value = jnp.dot(mixed, out_weight, preferred_element_type=jnp.float32).astype(
        jnp.bfloat16
    )
    partial_value = lax.optimization_barrier(partial_value).astype(jnp.float32)
    summed = of_everyone(partial_value.astype(jnp.bfloat16), "tp").astype(jnp.float32)
    residual = (tokens_float + summed).astype(jnp.bfloat16)
    expert_input = row_norm(residual.astype(jnp.float32)).astype(jnp.bfloat16)
    seq_count, top_count = route_experts.shape
    expert_count = lax.axis_size("ep")
    capacity = max(2, (2 * seq_count * top_count + expert_count - 1) // expert_count)
    column_count = expert_input.shape[1] // lax.axis_size("tp")
    column_start = lax.axis_index("tp") * column_count
    flat_routes = route_experts.reshape(-1)
    onehot = (flat_routes[:, None] == jnp.arange(expert_count, dtype=jnp.int32)[None, :]).astype(
        jnp.int32
    )
    earlier = jnp.cumsum(onehot, axis=0) - onehot
    target = flat_routes * capacity + jnp.sum(earlier * onehot, axis=1)
    slot_ids = jnp.arange(expert_count * capacity, dtype=jnp.int32)
    dispatch_map = jnp.any(
        slot_ids[:, None, None] == target.reshape(seq_count, top_count)[None], axis=-1
    )
    dispatch_map = dispatch_map.astype(jnp.bfloat16)
    outgoing = lax.dynamic_slice_in_dim(expert_input, column_start, column_count, 1)
    buffer = jnp.dot(dispatch_map, outgoing, preferred_element_type=jnp.float32).astype(
        jnp.bfloat16
    )
    buffer = buffer.reshape(expert_count, capacity, outgoing.shape[1])
    slot_rows = collect(
        lax.all_to_all(buffer, "ep", split_axis=0, concat_axis=0, tiled=True), "tp", 2
    )
    source_count, slot_count, model_width = slot_rows.shape
    flat_rows = slot_rows.reshape(-1, model_width)
    gate_pre = jnp.dot(flat_rows, expert_gate[0], preferred_element_type=jnp.float32)
    up_pre = jnp.dot(flat_rows, expert_up[0], preferred_element_type=jnp.float32)
    activated = clamped_unit(gate_pre, up_pre).astype(jnp.bfloat16)
    part_out = jnp.dot(activated, expert_down[0], preferred_element_type=jnp.float32).astype(
        jnp.bfloat16
    )
    part_out = lax.optimization_barrier(part_out).astype(jnp.float32)
    part_out = part_out.reshape(source_count, slot_count, model_width)
    shares = sum_at_owner(part_out.astype(jnp.bfloat16), "tp", 2).astype(jnp.bfloat16)
    returned = lax.all_to_all(shares, "ep", split_axis=0, concat_axis=0, tiled=True)
    picked = returned.reshape(expert_count * capacity, column_count)[target]
    picked = picked.reshape(seq_count, top_count, column_count).astype(jnp.float32)
    mixture = jnp.sum(route_weights[:, :, None] * picked, axis=1)
    own_residual = lax.dynamic_slice_in_dim(residual, column_start, column_count, 1).astype(
        jnp.float32
    )
    layer_out = (own_residual + mixture).astype(jnp.bfloat16)
    return (layer_out, new_state)


def solution(mesh):
    in_specs = (
        P("ep", None),
        P("ep", "tp", None, None),
        P(None, "tp"),
        P(None, "tp"),
        P(None, "tp"),
        P(),
        P(None, "tp"),
        P("tp"),
        P(),
        P(None, "tp"),
        P("tp"),
        P("tp"),
        P("tp", None),
        P("ep", None),
        P("ep", None),
        P("ep", None, "tp"),
        P("ep", None, "tp"),
        P("ep", "tp", None),
    )
    out_specs = (P("ep", "tp"), P("ep", "tp", None, None))
    return jax.shard_map(local, mesh=mesh, in_specs=in_specs, out_specs=out_specs, check_vma=False)
```

profile of v0, /device:TPU:1, one launch (start us, length us, event | category | flops | bytes accessed | tf_op | source)
XLA Modules:
  0.0 136.3 jit_solution(11909213838590096239)
XLA Ops:
  0.6 1.1 fusion.22
  1.7 1.2 fusion.10
  3.2 1.3 fusion.6
  4.7 1.4 fusion.39
  6.1 1.2 fusion.9
  7.4 1.2 convolution_convert_fusion.3
  8.9 2.9 %fusion.57 = f32[48,2,1,64]{3,2,1,0:T(1,128)S(1)} fusion(f32[48,2,64,1]{2,3,1,0:T(1,128)S(1)} %bitcast.63, f32[48,2,64,64]{3,2,1,0:T(8,128)} %param.19), kind=kOutput, calls=%fused_computation.91 | convolution fusion | flops 786432 | bytes 1622016 | tf_op jit(solution)/shard_map/shvk,shk->shv/dot_general | solution.py:69
  11.8 2.1 %multiply_add_fusion = f32[48,2,64,64]{3,2,1,0:T(8,128)S(1)} fusion(f32[48,2,64,64]{3,2,1,0:T(8,128)S(1)} %copy-done.1, f32[48,2,64]{2,1,0:T(2,128)S(1)} %get-tuple-element.6, f32[48,2,64]{2,1,0:T(2,128)S(1)} %reshape.152, f32[48,2,64]{2,1,0:T(2,128)S(1)} %get-tuple-element.4, f32[48,2,64]{2,1,0:T(2,128)S(1)} %bitcast.62, f32[48,2,64]{2,1,0:T(2,128)S(1)} %mul.155), kind=kLoop, calls=%fused_computation.1 | loop fusion | flops 1966080 | bytes 3268608 | tf_op jit(solution)/shard_map/add | solution.py:71
  13.9 1.7 %copy-done.2 = f32[48,2,64,64]{3,2,1,0:T(8,128)} copy-done((f32[48,2,64,64]{3,2,1,0:T(8,128)}, f32[48,2,64,64]{3,2,1,0:T(8,128)S(1)}, u32[]{:S(2)}) %copy-start.2) | copy-done | bytes 1572888
  15.6 0.9 fusion.58
  16.7 0.2 multiply_reduce_fusion.2
  16.9 0.2 subtract_multiply_fusion
  17.2 0.2 convolution_convert_fusion.2
  17.3 0.8 broadcast_in_dim.4
  18.1 5.0 %all-to-all-start = ((bf16[4,48,1024]{2,1,0:T(8,128)(2,1)}), bf16[4,48,1024]{2,1,0:T(8,128)(2,1)S(1)}, u32[]{:S(2)}, u32[]{:S(2)}) async-start(bf16[4,48,1024]{2,1,0:T(8,128)(2,1)} %broadcast_in_dim.4), calls=%async_computation | async-start | bytes 786432 | tf_op jit(solution)/shard_map/all_to_all | solution.py:15
  23.7 0.2 fusion.32
  24.2 5.2 %all-to-all-done = bf16[4,48,1024]{2,1,0:T(8,128)(2,1)S(1)} async-done(((bf16[4,48,1024]{2,1,0:T(8,128)(2,1)}), bf16[4,48,1024]{2,1,0:T(8,128)(2,1)S(1)}, u32[]{:S(2)}, u32[]{:S(2)}) %all-to-all-start) | async-done | bytes 393248 | tf_op jit(solution)/shard_map/all_to_all | solution.py:15
  29.6 0.3 convolution_convert_fusion.1
  30.0 41.9 %all_to_all.25 = bf16[128,3,256]{2,1,0:T(4,128)(2,1)S(1)} all-to-all(bf16[128,3,256]{2,1,0:T(4,128)(2,1)S(1)} %reshape.148), channel_id=1, replica_groups=mesh['ep'=128,'tp'=4] {'ep'}, dimensions={0} | all-to-all | bytes 393216 | tf_op jit(solution)/shard_map/all_to_all | solution.py:151
  72.0 14.4 %all_to_all.26 = bf16[4,128,3,256]{3,1,2,0:T(8,128)(2,1)S(1)} all-to-all(bf16[4,128,3,256]{3,1,2,0:T(8,128)(2,1)S(1)} %broadcast_in_dim.5), channel_id=1, replica_groups=mesh['ep'=128,'tp'=4] {'tp'}, dimensions={0} | all-to-all | bytes 1572864 | tf_op jit(solution)/shard_map/all_to_all | solution.py:15
  86.5 0.6 copy.81
  87.2 0.4 convolution_minimum_fusion
  87.6 1.0 convolution_convert_fusion
  88.6 0.6 convert_element_type.96
  89.3 13.1 %all_to_all.27 = bf16[4,128,3,256]{3,1,2,0:T(8,128)(2,1)S(1)} all-to-all(bf16[4,128,3,256]{3,1,2,0:T(8,128)(2,1)S(1)} %bitcast.52), channel_id=1, replica_groups=mesh['ep'=128,'tp'=4] {'tp'}, dimensions={0} | all-to-all | bytes 1572864 | tf_op jit(solution)/shard_map/all_to_all | solution.py:41
  102.7 0.9 copy.83
  103.5 10.3 %all-to-all-start.4 = ((bf16[128,3,256]{2,1,0:T(4,128)(2,1)}), bf16[128,3,256]{2,1,0:T(4,128)(2,1)S(1)}, u32[]{:S(2)}, u32[]{:S(2)}) async-start(bf16[128,3,256]{2,1,0:T(4,128)(2,1)} %copy.83), calls=%async_computation.4 | async-start | bytes 524288 | tf_op jit(solution)/shard_map/all_to_all | solution.py:164
  114.0 20.2 %all-to-all-done.4 = bf16[128,3,256]{2,1,0:T(4,128)(2,1)S(1)} async-done(((bf16[128,3,256]{2,1,0:T(4,128)(2,1)}), bf16[128,3,256]{2,1,0:T(4,128)(2,1)S(1)}, u32[]{:S(2)}, u32[]{:S(2)}) %all-to-all-start.4) | async-done | bytes 196640 | tf_op jit(solution)/shard_map/all_to_all | solution.py:164
  134.3 0.2 reshape.149
  134.4 1.0 gather_fusion
  135.5 0.2 multiply_reduce_fusion
  135.7 0.6 add_convert_fusion
  (62 shorter events, 2.9 us)
Async XLA Ops:
  0.6 87.0 %copy-start = (bf16[1,256,1024]{2,1,0:T(8,128)(2,1)S(1)}, bf16[1,256,1024]{2,1,0:T(8,128)(2,1)}, u32[]{:S(2)}) copy-start(bf16[1,256,1024]{2,1,0:T(8,128)(2,1)} %param.35) | copy-start | bytes 1572868
  8.8 3.1 %copy-start.1 = (f32[48,2,64,64]{3,2,1,0:T(8,128)S(1)}, f32[48,2,64,64]{3,2,1,0:T(8,128)}, u32[]{:S(2)}) copy-start(f32[48,2,64,64]{3,2,1,0:T(8,128)} %param.19) | copy-start | bytes 4718596
  13.9 1.7 %copy-start.2 = (f32[48,2,64,64]{3,2,1,0:T(8,128)}, f32[48,2,64,64]{3,2,1,0:T(8,128)S(1)}, u32[]{:S(2)}) copy-start(f32[48,2,64,64]{3,2,1,0:T(8,128)S(1)} %multiply_add_fusion) | copy-start | bytes 4718596
  15.6 1.6 %copy-start.5 = (bf16[128,1024]{1,0:T(8,128)(2,1)S(1)}, bf16[128,1024]{1,0:T(8,128)(2,1)}, u32[]{:S(2)}) copy-start(bf16[128,1024]{1,0:T(8,128)(2,1)} %param.30) | copy-start | bytes 786436
  15.6 1.6 %copy-start.8 = (f32[128]{0:T(128)S(1)}, f32[128]{0:T(128)}, u32[]{:S(2)}) copy-start(f32[128]{0:T(128)} %param.29) | copy-start | bytes 1540
  15.6 7.5 %copy-start.6 = (s32[48,4]{0,1:T(4,128)S(1)}, s32[48,4]{0,1:T(4,128)}, u32[]{:S(2)}) copy-start(s32[48,4]{0,1:T(4,128)} %param.31) | copy-start | bytes 2308
  15.6 13.8 %copy-start.3 = (bf16[48,1024]{1,0:T(8,128)(2,1)S(1)}, bf16[48,1024]{1,0:T(8,128)(2,1)}, u32[]{:S(2)}) copy-start(bf16[48,1024]{1,0:T(8,128)(2,1)} %param.18) | copy-start | bytes 294916
  18.1 11.2 %all-to-all-start = ((bf16[4,48,1024]{2,1,0:T(8,128)(2,1)}), bf16[4,48,1024]{2,1,0:T(8,128)(2,1)S(1)}, u32[]{:S(2)}, u32[]{:S(2)}) async-start(bf16[4,48,1024]{2,1,0:T(8,128)(2,1)} %broadcast_in_dim.4), calls=%async_computation | async-start | bytes 786432 | tf_op jit(solution)/shard_map/all_to_all | solution.py:15
  71.9 15.3 %copy-start.4 = (bf16[1,1024,256]{2,1,0:T(8,128)(2,1)S(1)}, bf16[1,1024,256]{2,1,0:T(8,128)(2,1)}, u32[]{:S(2)}) copy-start(bf16[1,1024,256]{2,1,0:T(8,128)(2,1)} %param.33) | copy-start | bytes 1572868
  72.0 15.6 %copy-start.9 = (bf16[1,1024,256]{2,1,0:T(8,128)(2,1)S(1)}, bf16[1,1024,256]{2,1,0:T(8,128)(2,1)}, u32[]{:S(2)}) copy-start(bf16[1,1024,256]{2,1,0:T(8,128)(2,1)} %param.34) | copy-start | bytes 1572868
  88.6 25.3 %copy-start.7 = (f32[48,4]{0,1:T(4,128)S(1)}, f32[48,4]{0,1:T(4,128)}, u32[]{:S(2)}) copy-start(f32[48,4]{0,1:T(4,128)} %param.32) | copy-start | bytes 2308
  103.5 30.8 %all-to-all-start.4 = ((bf16[128,3,256]{2,1,0:T(4,128)(2,1)}), bf16[128,3,256]{2,1,0:T(4,128)(2,1)S(1)}, u32[]{:S(2)}, u32[]{:S(2)}) async-start(bf16[128,3,256]{2,1,0:T(4,128)(2,1)} %copy.83), calls=%async_computation.4 | async-start | bytes 524288 | tf_op jit(solution)/shard_map/all_to_all | solution.py:164
where the time goes:
time: 138 us; the launch traced here: 136 us
  blocking collectives  69.5 us (50%)
  waiting for transfers between devices  25.4 us (18%)
  starting transfers between devices  15.3 us (11%)
  matrix products  12 us (9%)
  local copies, waits for them, and re-layouts  7.34 us (5%)
  other arithmetic  5.73 us (4%)
    all_to_all x1, blocking collectives, local(): lax.all_to_all(buffer, 'ep', split_axis=0, concat_axis=0, tiled=True)  41.9 us
    all_to_all x1, waiting for transfers between devices, local(): lax.all_to_all(shares, 'ep', split_axis=0, concat_axis=0, tiled=True)  20.2 us
    all_to_all x1, blocking collectives, copy_for_each(): lax.all_to_all(jnp.broadcast_to(value[None], (length, *value.shape)), axi...  14.4 us
    all_to_all x1, blocking collectives, sum_at_owner(): lax.all_to_all(cut_along(value, dim, length), axis, 0, 0, tiled=True)  13.1 us
    all_to_all x1, starting transfers between devices, local(): lax.all_to_all(shares, 'ep', split_axis=0, concat_axis=0, tiled=True)  10.3 us
    all_to_all x1, waiting for transfers between devices, copy_for_each(): lax.all_to_all(jnp.broadcast_to(value[None], (length, *value.shape)), axi...  5.17 us
    all_to_all x1, starting transfers between devices, copy_for_each(): lax.all_to_all(jnp.broadcast_to(value[None], (length, *value.shape)), axi...  5 us
    dot_general x1, matrix products, update_heads(): state_unit = jnp.einsum('shvk,shk->shv', head_state, unit_key)  2.94 us
  transfers between devices with their start and end apart: 2, of which 2 were waited for; matrix products, arithmetic and copies ran while one was open for 1% of the time, Pallas kernels for 0%

commit v1 on v0

v1 whole, which is shorter than its diff:
```python
import functools

import jax
import jax.numpy as jnp
from jax import lax
from jax.experimental import pallas as pl
from jax.experimental.pallas import tpu as pltpu
from jax.sharding import PartitionSpec as P

NORM_EPS = 1e-05
GROUP_EPS = 0.00064
UNIT_EPS = 1e-06
CLAMP_LIMIT = 7.0
GLU_ALPHA = 1.702
PLANE = 8
SLOTS = 3
LANES = 128
GROUP = 4
MESH = pl.DeviceIdType.MESH
F32, BF16, I32 = jnp.float32, jnp.bfloat16, jnp.int32


def plane_offset(j):
    half = (j + 1) // 2
    return half if j % 2 else -half


def row_norm(values):
    return values * lax.rsqrt(jnp.mean(values * values, axis=-1, keepdims=True) + NORM_EPS)


def update_heads(head_state, recept, keys, values, decay_rate, rate_gate, head_gain):
    seq_count, head_count, head_size = head_state.shape[:3]

    def by_heads(operand):
        return operand.astype(jnp.float32).reshape(seq_count, head_count, head_size)

    recept_heads = by_heads(recept)
    key_heads = by_heads(keys)
    value_heads = by_heads(values)
    decay_heads = by_heads(decay_rate)
    rate_heads = by_heads(rate_gate)
    unit_key = key_heads * lax.rsqrt(
        jnp.sum(key_heads * key_heads, axis=-1, keepdims=True) + UNIT_EPS
    )
    state_unit = jnp.einsum("shvk,shk->shv", head_state, unit_key)
    new_state = (
        head_state * decay_heads[:, :, None, :]
        - state_unit[..., None] * (unit_key * rate_heads)[:, :, None, :]
        + value_heads[..., None] * (key_heads * rate_heads)[:, :, None, :]
    )
    head_out = jnp.einsum("shvk,shk->shv", new_state, recept_heads)
    centre = jnp.mean(head_out, axis=-1, keepdims=True)
    spread = jnp.mean(jnp.square(head_out - centre), axis=-1, keepdims=True)
    normed_heads = (head_out - centre) * lax.rsqrt(spread + GROUP_EPS)
    mixed = (normed_heads.reshape(seq_count, -1) * head_gain).astype(jnp.bfloat16)
    return (new_state, mixed)


def expert_kernel(
    sizes,
    partial_ref,
    tokens_ref,
    routes_ref,
    weights_ref,
    gate_ref,
    up_ref,
    down_ref,
    out_ref,
    gu_vm,
    down_vm,
    info_out,
    info_in,
    part_in,
    resid,
    pick,
    mix_hi,
    mix_lo,
    z_out,
    z_in,
    y_in,
    share_out,
    share_in,
    back_out,
    back_in,
    mix_out,
    mix_in,
    load_sem,
    info_send,
    info_recv,
    part_send,
    part_recv,
    res_send,
    res_recv,
    z_send,
    z_recv,
    y_send,
    y_recv,
    share_send,
    share_recv,
    back_send,
    back_recv,
    mix_send,
    mix_recv,
):
    nz, nk, ny, seqs, width = sizes
    half = width // 2
    block = SLOTS * nk
    rows = nz * block
    groups = [range(g, min(g + GROUP, nz)) for g in range(0, nz, GROUP)]
    ep = lax.axis_index("ep")
    y = lax.axis_index("tp")
    z, k = ep // nk, ep % nk

    def in_z(j):
        return ((z + (plane_offset(j) + nz)) % nz) * nk + k, y

    def out_z(j):
        return ((z + (nz - plane_offset(j))) % nz) * nk + k, y

    def in_plane(q):
        return z * nk + (k + q) % nk, y

    def back_plane(q):
        return z * nk + (k + (nk - q)) % nk, y

    def in_y(q):
        return ep, (y + q) % ny

    def send(source, target, sends, receives, device):
        copy = pltpu.make_async_remote_copy(
            src_ref=source,
            dst_ref=target,
            send_sem=sends,
            recv_sem=receives,
            device_id=device,
            device_id_type=MESH,
        )
        copy.start()
        return copy

    barrier = pltpu.get_barrier_semaphore()
    peers = (
        [in_y(q) for q in range(1, ny)]
        + [in_plane(q) for q in range(1, nk)]
        + [in_z(j) for j in range(1, nz)]
    )
    for device in peers:
        pl.semaphore_signal(barrier, inc=1, device_id=device, device_id_type=MESH)

    loads = []
    for q in range(ny):
        own = pl.ds(pl.multiple_of(((y + (ny - q)) % ny) * width, LANES), width)
        put = pl.ds(q * width, width)
        hidden = gate_ref.shape[2]
        loads.append(
            pltpu.make_async_copy(
                gate_ref.at[0, own, :], gu_vm.at[put, pl.ds(0, hidden)], load_sem.at[0, q]
            )
        )
        loads.append(
            pltpu.make_async_copy(
                up_ref.at[0, own, :], gu_vm.at[put, pl.ds(hidden, hidden)], load_sem.at[1, q]
            )
        )
        ahead = pl.ds(pl.multiple_of(((y + q) % ny) * width, LANES), width)
        loads.append(
            pltpu.make_async_copy(
                down_ref.at[0, :, ahead], down_vm.at[:, pl.ds(q * width, width)], load_sem.at[2, q]
            )
        )
    for load in loads:
        load.start()

    count = nk * nz
    row = lax.broadcasted_iota(I32, (count, LANES), 0)
    j_of, q_of = row % nz, row // nz
    far = (j_of + 1) // 2
    away = jnp.where(j_of % 2 == 1, far, nz - far)
    expert = ((z + away) % nz) * nk + (k + q_of) % nk
    member = jnp.zeros((count, LANES), F32)
    weight = jnp.zeros((count, LANES), F32)
    for c in range(4):
        named = routes_ref[c : c + 1, :] == expert
        member = member + jnp.where(named, 1.0, 0.0)
        weight = weight + jnp.where(named, weights_ref[c : c + 1, :], 0.0)
    earlier_row = lax.broadcasted_iota(I32, (LANES, LANES), 0)
    later_row = lax.broadcasted_iota(I32, (LANES, LANES), 1)
    before = jnp.where(earlier_row < later_row, 1.0, 0.0).astype(BF16)
    earlier = jnp.dot(member.astype(BF16), before, preferred_element_type=F32)
    code = jnp.where(member > 0.5, earlier, 9.0)
    for q in range(nk):
        info_out[q, 0:nz, :] = code[q * nz : (q + 1) * nz]
        info_out[q, nz : 2 * nz, :] = weight[q * nz : (q + 1) * nz]

    resid[:, seqs:, :] = jnp.zeros((nk, LANES - seqs, width), BF16)

    pl.semaphore_wait(barrier, len(peers))

    flights = []
    arriving = {}
    for q in range(1, ny):
        copy = send(
            partial_ref.at[(y + q) % ny], part_in.at[q], part_send.at[q], part_recv.at[q], in_y(q)
        )
        arriving["part", q] = copy
        flights.append(copy)
    for q in range(1, nk):
        copy = send(info_out.at[q], info_in.at[q], info_send.at[q], info_recv.at[q], in_plane(q))
        arriving["info", q] = copy
        flights.append(copy)

    summed = partial_ref[y].astype(F32)
    for q in range(1, ny):
        arriving["part", q].wait_recv()
        summed = summed + part_in[q].astype(F32)
    residual = (tokens_ref[y].astype(F32) + summed).astype(BF16)
    resid[0, 0:seqs, :] = residual
    for q in range(1, nk):
        copy = send(
            resid.at[0, pl.ds(0, seqs)],
            resid.at[q, pl.ds(0, seqs)],
            res_send.at[q],
            res_recv.at[q],
            in_plane(q),
        )
        arriving["res", q] = copy
        flights.append(copy)

    rep_row = lax.broadcasted_iota(I32, (nz, SLOTS, nk, nz), 0).reshape(rows, nz)
    rep_col = lax.broadcasted_iota(I32, (nz, SLOTS, nk, nz), 3).reshape(rows, nz)
    repeat = jnp.where(rep_row == rep_col, 1.0, 0.0).astype(BF16)
    slot = lax.broadcasted_iota(I32, (nz, SLOTS, nk, LANES), 1).reshape(rows, LANES).astype(F32)
    source = lax.broadcasted_iota(I32, (nz, SLOTS, nk, LANES), 2).reshape(rows, LANES)
    for q in range(nk):
        if q:
            arriving["info", q].wait_recv()
        told = info_out if q == 0 else info_in
        spread = jnp.dot(repeat, told[q, 0:nz, :].astype(BF16), preferred_element_type=F32)
        chosen = jnp.where(spread == slot, jnp.where(source == q, 1.0, 0.0), 0.0)
        pick[:, q * LANES : (q + 1) * LANES] = chosen.astype(BF16)

    for q in range(1, nk):
        arriving["res", q].wait_recv()
    outgoing = jnp.dot(
        pick[...], resid[...].reshape(nk * LANES, width), preferred_element_type=F32
    ).reshape(nz, block, width)
    z_out[...] = jnp.concatenate([outgoing[:, :, :half], outgoing[:, :, half:]], axis=1).astype(BF16)

    for j in range(1, nz):
        copy = send(z_out.at[j], z_in.at[j], z_send.at[j], z_recv.at[j], in_z(j))
        arriving["z", j] = copy
        flights.append(copy)

    for q in range(nk):
        told = info_out if q == 0 else info_in
        weight = told[q, nz : 2 * nz, :]
        high = weight.astype(BF16)
        low = (weight - high.astype(F32)).astype(BF16)
        spread = jnp.dot(repeat, high, preferred_element_type=F32) + jnp.dot(
            repeat, low, preferred_element_type=F32
        )
        scaled = (spread * pick[:, q * LANES : (q + 1) * LANES].astype(F32)).T[0:seqs, :]
        high = scaled.astype(BF16)
        mix_hi[q] = high
        mix_lo[q] = (scaled - high.astype(F32)).astype(BF16)

    def forward(j):
        held = z_out.at[0] if j == 0 else z_in.at[j]
        if j:
            arriving["z", j].wait_recv()
        for q in range(1, ny):
            copy = send(held, y_in.at[q, j], y_send.at[q, j], y_recv.at[q, j], in_y(q))
            arriving["y", q, j] = copy
            flights.append(copy)

    def experts(group):
        columns = []
        for q in range(ny):
            pieces = []
            for j in group:
                if q:
                    arriving["y", q, j].wait_recv()
                    held = y_in[q, j]
                elif j:
                    held = z_in[j]
                else:
                    held = z_out[0]
                held = held.astype(F32)
                pieces.append(jnp.concatenate([held[:block], held[block:]], axis=1))
            columns.append(jnp.concatenate(pieces, axis=0))
        features = jnp.concatenate(columns, axis=1)
        normed = row_norm(features).astype(BF16)
        hidden = gu_vm.shape[1] // 2
        pre = jnp.dot(normed, gu_vm[...], preferred_element_type=F32)
        gated = jnp.minimum(pre[:, :hidden], CLAMP_LIMIT)
        linear = jnp.clip(pre[:, hidden:], -CLAMP_LIMIT, CLAMP_LIMIT)
        activated = (gated * jax.nn.sigmoid(GLU_ALPHA * gated) * (linear + 1.0)).astype(BF16)
        share = jnp.dot(activated, down_vm[...], preferred_element_type=F32)
        for q in range(ny):
            for at, j in enumerate(group):
                piece = share[at * block : (at + 1) * block, q * width : (q + 1) * width]
                share_out[q, j] = jnp.concatenate([piece[:, :half], piece[:, half:]], axis=0).astype(
                    BF16
                )
        for j in group:
            for q in range(1, ny):
                copy = send(
                    share_out.at[q, j],
                    share_in.at[q, j],
                    share_send.at[q, j],
                    share_recv.at[q, j],
                    in_y(q),
                )
                arriving["share", q, j] = copy
                flights.append(copy)

    def give_back(group):
        for j in group:
            total = share_out[0, j].astype(F32)
            for q in range(1, ny):
                arriving["share", q, j].wait_recv()
                total = total + share_in[q, j].astype(F32)
            total = total.astype(BF16)
            if j:
                back_out[j] = total
                copy = send(back_out.at[j], back_in.at[j], back_send.at[j], back_recv.at[j], out_z(j))
                arriving["back", j] = copy
                flights.append(copy)
            else:
                back_in[0] = total

    for g, group in enumerate(groups):
        for j in group:
            forward(j)
        if g == 0:
            for load in loads:
                load.wait()
        if g >= 1:
            experts(groups[g - 1])
        if g >= 2:
            give_back(groups[g - 2])
    experts(groups[-1])
    for group in groups[max(0, len(groups) - 2) :]:
        give_back(group)

    for j in range(1, nz):
        arriving["back", j].wait_recv()
    returned = back_in[...].astype(F32)
    returned = jnp.concatenate([returned[:, :block], returned[:, block:]], axis=2)
    returned = returned.reshape(rows, width).astype(BF16)
    mixture = jnp.dot(
        mix_hi[...].reshape(nk * seqs, rows), returned, preferred_element_type=F32
    ) + jnp.dot(mix_lo[...].reshape(nk * seqs, rows), returned, preferred_element_type=F32)
    mix_out[...] = mixture.reshape(nk, seqs, width).astype(BF16)
    for q in range(1, nk):
        copy = send(mix_out.at[q], mix_in.at[q], mix_send.at[q], mix_recv.at[q], back_plane(q))
        arriving["mix", q] = copy
        flights.append(copy)
    total = mixture[0:seqs]
    for q in range(1, nk):
        arriving["mix", q].wait_recv()
        total = total + mix_in[q].astype(F32)
    out_ref[...] = (resid[0, 0:seqs, :].astype(F32) + total).astype(BF16)
    for copy in flights:
        copy.wait_send()


def run_experts(sizes, partial, tokens, routes, weights, gate, up, down):
    nz, nk, ny, seqs, width = sizes
    rows = nz * SLOTS * nk
    message = (2 * SLOTS * nk, width // 2)
    hidden = gate.shape[2]
    dma = pltpu.SemaphoreType.DMA
    vmem = pl.BlockSpec(memory_space=pltpu.VMEM)
    hbm = pl.BlockSpec(memory_space=pl.ANY)
    scratch = [
        pltpu.VMEM((ny * width, 2 * hidden), BF16),
        pltpu.VMEM((hidden, ny * width), BF16),
        pltpu.VMEM((nk, 2 * nz, LANES), F32),
        pltpu.VMEM((nk, 2 * nz, LANES), F32),
        pltpu.VMEM((ny, seqs, width), BF16),
        pltpu.VMEM((nk, LANES, width), BF16),
        pltpu.VMEM((rows, nk * LANES), BF16),
        pltpu.VMEM((nk, seqs, rows), BF16),
        pltpu.VMEM((nk, seqs, rows), BF16),
        pltpu.VMEM((nz, *message), BF16),
        pltpu.VMEM((nz, *message), BF16),
        pltpu.VMEM((ny, nz, *message), BF16),
        pltpu.VMEM((ny, nz, *message), BF16),
        pltpu.VMEM((ny, nz, *message), BF16),
        pltpu.VMEM((nz, *message), BF16),
        pltpu.VMEM((nz, *message), BF16),
        pltpu.VMEM((nk, seqs, width), BF16),
        pltpu.VMEM((nk, seqs, width), BF16),
        dma((3, ny)),
    ]
    for shape in ((nk,), (ny,), (nk,), (nz,), (ny, nz), (ny, nz), (nz,), (nk,)):
        scratch += [dma(shape), dma(shape)]
    return pl.pallas_call(
        functools.partial(expert_kernel, sizes),
        out_shape=jax.ShapeDtypeStruct((seqs, width), BF16),
        in_specs=[vmem] * 4 + [hbm] * 3,
        out_specs=vmem,
        scratch_shapes=scratch,
        compiler_params=pltpu.CompilerParams(
            collective_id=0, has_side_effects=True, vmem_limit_bytes=40 * 1024 * 1024
        ),
        name="experts",
    )(partial, tokens, routes, weights, gate, up, down)


def local(
    tokens,
    head_state,
    recept_weight,
    key_weight,
    value_weight,
    decay_down_factor,
    decay_up_factor,
    decay_base,
    rate_down_factor,
    rate_up_factor,
    rate_base,
    head_gain,
    out_weight,
    route_experts,
    route_weights,
    expert_gate,
    expert_up,
    expert_down,
):
    tokens_float = tokens.astype(jnp.float32)
    normed = row_norm(tokens_float).astype(jnp.bfloat16)
    recept = jnp.dot(normed, recept_weight, preferred_element_type=jnp.float32).astype(jnp.bfloat16)
    keys = jnp.dot(normed, key_weight, preferred_element_type=jnp.float32).astype(jnp.bfloat16)
    values = jnp.dot(normed, value_weight, preferred_element_type=jnp.float32).astype(jnp.bfloat16)
    decay_low = jnp.tanh(
        jnp.dot(normed, decay_down_factor, preferred_element_type=jnp.float32)
    ).astype(jnp.bfloat16)
    rate_low = jnp.dot(normed, rate_down_factor, preferred_element_type=jnp.float32).astype(
        jnp.bfloat16
    )
    decay_pre = decay_base + jnp.dot(decay_low, decay_up_factor, preferred_element_type=jnp.float32)
    decay_rate = jnp.exp(-jnp.exp(-jax.nn.softplus(-decay_pre) - 0.5))
    rate_gate = jax.nn.sigmoid(
        rate_base + jnp.dot(rate_low, rate_up_factor, preferred_element_type=jnp.float32)
    )
    new_state, mixed = update_heads(
        head_state, recept, keys, values, decay_rate, rate_gate, head_gain
    )
    partial_value = jnp.dot(mixed, out_weight, preferred_element_type=jnp.float32).astype(
        jnp.bfloat16
    )
    ny = lax.axis_size("tp")
    nz = lax.axis_size("ep") // PLANE
    seqs, model = tokens.shape
    width = model // ny

    def by_columns(value):
        return value.reshape(seqs, ny, width).transpose(1, 0, 2)

    def by_lanes(value, fill):
        return jnp.pad(
            value.T, ((0, 8 - value.shape[1]), (0, LANES - seqs)), constant_values=fill
        )

    layer_out = run_experts(
        (nz, PLANE, ny, seqs, width),
        by_columns(partial_value),
        by_columns(tokens),
        by_lanes(route_experts, -1),
        by_lanes(route_weights, 0.0),
        expert_gate,
        expert_up,
        expert_down,
    )
    return (layer_out, new_state)


def solution(mesh):
    in_specs = (
        P("ep", None),
        P("ep", "tp", None, None),
        P(None, "tp"),
        P(None, "tp"),
        P(None, "tp"),
        P(),
        P(None, "tp"),
        P("tp"),
        P(),
        P(None, "tp"),
        P("tp"),
        P("tp"),
        P("tp", None),
        P("ep", None),
        P("ep", None),
        P("ep", None, "tp"),
        P("ep", None, "tp"),
        P("ep", "tp", None),
    )
    out_specs = (P("ep", "tp"), P("ep", "tp", None, None))
    return jax.shard_map(local, mesh=mesh, in_specs=in_specs, out_specs=out_specs, check_vma=False)
```

time: 138 us -> 96.4 us (0.70)
  blocking collectives: 69.5 us -> 0 us
  Pallas kernels: 0 us -> 66.4 us
  waiting for transfers between devices: 25.4 us -> 0 us
  starting transfers between devices: 15.3 us -> 0 us
  other arithmetic: 5.73 us -> 8.27 us
  matrix products: 12 us -> 14.3 us
  local copies, waits for them, and re-layouts: 7.34 us -> 5.92 us
    all_to_all x3 -> x0, blocking collectives: 69.5 us -> none  [the longest x1 41.9 us: local(): lax.all_to_all(buffer, 'ep', split_axis=0, concat_axis=0, tiled=True)]
    pallas_call x0 -> x1, Pallas kernels: none -> 66.4 us  [run_experts(): pl.pallas_call(functools.partial(expert_kernel, sizes), out_shape=jax.Sha...]
    all_to_all x2 -> x0, waiting for transfers between devices: 25.4 us -> none  [the longest x1 20.2 us: local(): lax.all_to_all(shares, 'ep', split_axis=0, concat_axis=0, tiled=True)]
    all_to_all x2 -> x0, starting transfers between devices: 15.3 us -> none  [the longest x1 10.3 us: local(): lax.all_to_all(shares, 'ep', split_axis=0, concat_axis=0, tiled=True)]
    add x1, other arithmetic: 2.07 us -> 4.3 us  [update_heads(): head_state * decay_heads[:, :, None, :]]
    reshape x3, local copies, waits for them, and re-layouts: 0.27 us -> 2.36 us  [by_heads(): return operand.astype(jnp.float32).reshape(seq_count, head_count, head_size)]
    dot_general x1, matrix products: 0.9 us -> 2.92 us  [update_heads(): head_out = jnp.einsum('shvk,shk->shv', new_state, recept_heads)]
    dot_general x3 -> x0, matrix products: 1.64 us -> none  [the longest x1 0.99 us: local(): jnp.dot(activated, expert_down[0], preferred_element_type=jnp.float32)]
  transfers between devices with their start and end apart: 2 -> 0, of which waited for: 2 -> 0; matrix products, arithmetic and copies ran while one was open for 1% -> 0% of each run, Pallas kernels for 0% -> 0%
where the time goes in v1:
time: 96.4 us; the launch traced here: 95.7 us
  Pallas kernels  66.4 us (69%)
  matrix products  14.3 us (15%)
  other arithmetic  8.27 us (9%)
  local copies, waits for them, and re-layouts  5.92 us (6%)
    pallas_call x1, Pallas kernels, run_experts(): pl.pallas_call(functools.partial(expert_kernel, sizes), out_shape=jax.Sha...  66.4 us
    add x1, other arithmetic, update_heads(): head_state * decay_heads[:, :, None, :]  4.3 us
    dot_general x1, matrix products, update_heads(): state_unit = jnp.einsum('shvk,shk->shv', head_state, unit_key)  3.45 us
    dot_general x1, matrix products, update_heads(): head_out = jnp.einsum('shvk,shk->shv', new_state, recept_heads)  2.92 us
    reshape x3, local copies, waits for them, and re-layouts, by_heads(): return operand.astype(jnp.float32).reshape(seq_count, head_count, head_size)  2.36 us
    dot_general x1, matrix products, local(): jnp.dot(rate_low, rate_up_factor, preferred_element_type=jnp.float32)  1.95 us

profile of v1, /device:TPU:1, one launch (start us, length us, event | category | flops | bytes accessed | tf_op | source)
XLA Modules:
  0.0 95.7 jit_solution(6073120403551365339)
XLA Ops:
  0.6 0.0 copy-start
  0.6 0.0 copy-start.5
  0.7 0.0 copy-start.4
  0.7 1.2 %fusion.8 = f32[48]{0:T(128)S(1)} fusion(bf16[48,1024]{1,0:T(8,128)(2,1)} %param.18), kind=kLoop, calls=%fused_computation.19 | loop fusion | flops 147408 | bytes 98496 | tf_op jit(solution)/shard_map/reduce_sum | solution.py:29
  1.9 0.5 copy-done.7
  2.3 1.8 %fusion.7 = f32[48,128]{1,0:T(8,128)} fusion(bf16[1024,128]{1,0:T(8,128)(2,1)} %param.21, bf16[48,1024]{1,0:T(8,128)(2,1)} %param.18, f32[48]{0:T(128)S(1)} %add_rsqrt_fusion.2), kind=kOutput, calls=%fused_computation.16 | convolution fusion | flops 12742656 | bytes 385216 | tf_op jit(solution)/shard_map/dot_general | solution.py:436
  4.2 0.8 reshape.84
  5.0 0.1 multiply_reduce_fusion.1
  5.1 0.6 add_rsqrt_fusion.1
  5.8 2.0 %fusion.3 = f32[48,128]{1,0:T(8,128)} fusion(bf16[64,128]{1,0:T(8,128)(2,1)} %param.27, bf16[1024,64]{0,1:T(8,128)(2,1)} %param.26, f32[128]{0:T(128)} %param.28, bf16[48,1024]{1,0:T(8,128)(2,1)} %param.18, f32[48]{0:T(128)} %copy-done.7), kind=kOutput, calls=%fused_computation.6 | convolution fusion | flops 7252992 | bytes 271040 | tf_op jit(solution)/shard_map/dot_general | solution.py:447
  7.7 1.4 %reshape.78 = f32[48,2,64]{2,1,0:T(2,128)} reshape(f32[48,128]{1,0:T(8,128)} %fusion.3) | data formatting | bytes 49152 | tf_op jit(solution)/shard_map/reshape | solution.py:36
  9.2 1.5 %fusion.23 = (f32[48,2,64]{2,1,0:T(2,128)}, f32[48,2,64]{2,1,0:T(2,128)S(1)}, f32[48,2,64]{2,1,0:T(2,128)}) fusion(f32[48,2,64]{2,1,0:T(2,128)} %reshape.78, f32[48,2,64]{2,1,0:T(2,128)S(1)} %reshape.84, f32[48,2]{1,0:T(8,128)} %add_rsqrt_fusion.1), kind=kLoop, calls=%fused_computation.39 | loop fusion | flops 18432 | bytes 123264 | tf_op jit(solution)/shard_map/mul | solution.py:49
  10.7 3.5 %fusion.24 = f32[48,2,1,64]{3,2,1,0:T(1,128)} fusion(f32[48,2,64,1]{2,3,1,0:T(1,128)S(1)} %bitcast.37, f32[48,2,64,64]{3,2,1,0:T(8,128)} %param.19), kind=kOutput, calls=%fused_computation.40 | convolution fusion | flops 786432 | bytes 1622016 | tf_op jit(solution)/shard_map/shvk,shk->shv/dot_general | solution.py:46
  14.2 1.9 %fusion.14 = f32[48,128]{1,0:T(8,128)} fusion(bf16[64,128]{1,0:T(8,128)(2,1)S(1)} %copy-done.13, bf16[1024,64]{0,1:T(8,128)(2,1)} %param.23, f32[128]{0:T(128)S(1)} %copy-done.14, bf16[48,1024]{1,0:T(8,128)(2,1)S(1)} %copy-done.5, f32[48]{0:T(128)S(1)} %copy-done.8), kind=kOutput, calls=%fused_computation.31 | convolution fusion | flops 7296000 | bytes 271040 | tf_op jit(solution)/shard_map/dot_general | solution.py:444
  16.1 0.8 mul.100
  16.9 1.8 %fusion.6 = f32[48,128]{1,0:T(8,128)} fusion(bf16[1024,128]{1,0:T(8,128)(2,1)} %param.22, bf16[48,1024]{1,0:T(8,128)(2,1)S(1)} %copy-done.5, f32[48]{0:T(128)} %copy-done.7), kind=kOutput, calls=%fused_computation.13 | convolution fusion | flops 12742656 | bytes 385216 | tf_op jit(solution)/shard_map/dot_general | solution.py:437
  18.7 1.4 %reshape.85 = f32[48,2,64]{2,1,0:T(2,128)} reshape(f32[48,128]{1,0:T(8,128)} %fusion.6) | data formatting | bytes 49152 | tf_op jit(solution)/shard_map/mul | solution.py:50
  20.2 4.3 %multiply_add_fusion = f32[48,2,64,64]{3,2,1,0:T(8,128)} fusion(f32[48,2,64,64]{3,2,1,0:T(8,128)S(1)} %copy-done.4, f32[48,2,64]{2,1,0:T(2,128)} %get-tuple-element.4, f32[48,2,64]{2,1,0:T(2,128)} %reshape.85, f32[48,2,64]{2,1,0:T(2,128)} %get-tuple-element.2, f32[48,2,64]{2,1,0:T(2,128)} %bitcast.36, f32[48,2,64]{2,1,0:T(2,128)S(1)} %mul.100), kind=kLoop, calls=%fused_computation | loop fusion | flops 1966080 | bytes 3268608 | tf_op jit(solution)/shard_map/add | solution.py:48
  24.5 0.0 copy-start.12
  24.5 0.0 copy-start.10
  24.5 0.0 copy-start.1
  24.5 0.0 copy-start.2
  24.5 0.2 convolution_convert_fusion.1
  24.8 0.1 reshape.91
  24.9 2.9 %fusion.25 = f32[48,2,1,64]{3,2,1,0:T(1,128)S(1)} fusion(f32[48,2,64,64]{3,2,1,0:T(8,128)} %multiply_add_fusion, bf16[48,2,64,1]{2,3,1,0:T(2,128)(2,1)S(1)} %reshape.91), kind=kOutput, calls=%fused_computation.41 | convolution fusion | flops 786432 | bytes 1609728 | tf_op jit(solution)/shard_map/shvk,shk->shv/dot_general | solution.py:52
  27.8 0.1 reduce_sum.38
  27.9 0.2 multiply_reduce_fusion
  28.2 0.2 subtract_multiply_fusion
  28.3 0.1 reshape.80
  28.4 0.2 convolution_convert_fusion
  28.7 66.4 %experts.1 = bf16[48,256]{1,0:T(8,128)(2,1)S(1)} custom-call(bf16[4,48,256]{2,1,0:T(8,128)(2,1)S(1)} %get-tuple-element.6.partial_ref, bf16[4,48,256]{2,1,0:T(8,128)(2,1)S(1)} %get-tuple-element.5.tokens_ref, s32[8,128]{1,0:T(8,128)S(1)} %pad.8.routes_ref, f32[8,128]{1,0:T(8,128)S(1)} %pad.9.weights_ref, bf16[1,1024,256]{2,1,0:T(8,128)(2,1)S(1)} %copy-done.1, ...), custom_call_target="tpu_custom_call" | custom-call | tf_op jit(solution)/shard_map/experts/pallas_call | solution.py:400
  95.1 0.6 copy.43
  (28 shorter events, 0.1 us)
Async XLA Ops:
  0.6 27.8 %copy-start = (bf16[128,1024]{1,0:T(8,128)(2,1)S(1)}, bf16[128,1024]{1,0:T(8,128)(2,1)}, u32[]{:S(2)}) copy-start(bf16[128,1024]{1,0:T(8,128)(2,1)} %param.30) | copy-start | bytes 786436
  0.6 13.5 %copy-start.5 = (bf16[48,1024]{1,0:T(8,128)(2,1)S(1)}, bf16[48,1024]{1,0:T(8,128)(2,1)}, u32[]{:S(2)}) copy-start(bf16[48,1024]{1,0:T(8,128)(2,1)} %param.18) | copy-start | bytes 294916
  0.7 19.5 %copy-start.4 = (f32[48,2,64,64]{3,2,1,0:T(8,128)S(1)}, f32[48,2,64,64]{3,2,1,0:T(8,128)}, u32[]{:S(2)}) copy-start(f32[48,2,64,64]{3,2,1,0:T(8,128)} %param.19) | copy-start | bytes 4718596
  1.8 0.5 copy-start.7
  10.7 3.5 %copy-start.8 = (f32[48]{0:T(128)S(1)}, f32[48]{0:T(128)}, u32[]{:S(2)}) copy-start(f32[48]{0:T(128)} %copy-done.7) | copy-start | bytes 580
  10.7 3.5 %copy-start.13 = (bf16[64,128]{1,0:T(8,128)(2,1)S(1)}, bf16[64,128]{1,0:T(8,128)(2,1)}, u32[]{:S(2)}) copy-start(bf16[64,128]{1,0:T(8,128)(2,1)} %param.24) | copy-start | bytes 49156
  10.7 3.5 %copy-start.14 = (f32[128]{0:T(128)S(1)}, f32[128]{0:T(128)}, u32[]{:S(2)}) copy-start(f32[128]{0:T(128)} %param.25) | copy-start | bytes 1540
  20.2 4.3 %copy-start.6 = (bf16[1024,128]{1,0:T(8,128)(2,1)S(1)}, bf16[1024,128]{1,0:T(8,128)(2,1)}, u32[]{:S(2)}) copy-start(bf16[1024,128]{1,0:T(8,128)(2,1)} %param.20) | copy-start | bytes 786436
  20.2 4.3 %copy-start.9 = (f32[48]{0:T(128)S(1)}, f32[48]{0:T(128)}, u32[]{:S(2)}) copy-start(f32[48]{0:T(128)} %copy-done.7) | copy-start | bytes 580
  24.5 4.0 %copy-start.12 = (f32[128]{0:T(128)S(1)}, f32[128]{0:T(128)}, u32[]{:S(2)}) copy-start(f32[128]{0:T(128)} %param.29) | copy-start | bytes 1540
  24.5 4.2 %copy-start.10 = (s32[48,4]{0,1:T(4,128)S(1)}, s32[48,4]{0,1:T(4,128)}, u32[]{:S(2)}) copy-start(s32[48,4]{0,1:T(4,128)} %param.31) | copy-start | bytes 2308
  24.5 4.2 %copy-start.11 = (f32[48,4]{0,1:T(4,128)S(1)}, f32[48,4]{0,1:T(4,128)}, u32[]{:S(2)}) copy-start(f32[48,4]{0,1:T(4,128)} %param.32) | copy-start | bytes 2308
  24.5 4.2 %copy-start.1 = (bf16[1,1024,256]{2,1,0:T(8,128)(2,1)S(1)}, bf16[1,1024,256]{2,1,0:T(8,128)(2,1)}, u32[]{:S(2)}) copy-start(bf16[1,1024,256]{2,1,0:T(8,128)(2,1)} %gate_ref.1) | copy-start | bytes 1572868
  24.5 4.2 %copy-start.2 = (bf16[1,1024,256]{2,1,0:T(8,128)(2,1)S(1)}, bf16[1,1024,256]{2,1,0:T(8,128)(2,1)}, u32[]{:S(2)}) copy-start(bf16[1,1024,256]{2,1,0:T(8,128)(2,1)} %up_ref.1) | copy-start | bytes 1572868
  24.5 4.2 %copy-start.3 = (bf16[1,256,1024]{2,1,0:T(8,128)(2,1)S(1)}, bf16[1,256,1024]{2,1,0:T(8,128)(2,1)}, u32[]{:S(2)}) copy-start(bf16[1,256,1024]{2,1,0:T(8,128)(2,1)} %down_ref.1) | copy-start | bytes 1572868

commit v2 on v0

v2 whole, which is shorter than its diff:
```python
import contextlib
import functools
import types

import jax
import jax.numpy as jnp
from jax import lax
from jax.experimental import pallas as pl
from jax.experimental.pallas import tpu as pltpu
from jax.sharding import PartitionSpec as P

NORM_EPS = 1e-05
GROUP_EPS = 0.00064
UNIT_EPS = 1e-06
CLAMP_LIMIT = 7.0
GLU_ALPHA = 1.702
PLANE = 8
SLOTS = 3
LANES = 128
GROUP = 4
PIECES = 6
SCOPES = False
MESH = pl.DeviceIdType.MESH
F32, BF16, I32 = jnp.float32, jnp.bfloat16, jnp.int32


def plane_offsets(nz):
    if nz == 16:
        return [0, 1, -1, 2, -2, 3, -3, 8, 7, -7, 6, -6, 5, -5, 4, -4]
    return [0] + [way * d for d in range(1, nz // 2) for way in (1, -1)] + [nz // 2]


def send_order(nz):
    offsets = plane_offsets(nz)
    ranked = sorted(range(1, nz), key=lambda j: -abs(offsets[j]))
    order = []
    while ranked:
        order.append(ranked.pop(0))
        if ranked:
            order.append(ranked.pop())
    return order


def scope(name):
    return jax.named_scope(name) if SCOPES else contextlib.nullcontext()


def row_norm(values):
    return values * lax.rsqrt(jnp.mean(values * values, axis=-1, keepdims=True) + NORM_EPS)


def dot(a, b):
    return jnp.dot(a, b, preferred_element_type=F32)


def dot_last(a, b):
    return lax.dot_general(a, b, (((1,), (1,)), ((), ())), preferred_element_type=F32)


INPUTS = [
    "tokens",
    "state",
    "recept",
    "key",
    "value",
    "decay_down",
    "decay_up",
    "decay_base",
    "rate_down",
    "rate_up",
    "rate_base",
    "gain",
    "out_weight",
    "routes",
    "weights",
    "gate",
    "up",
    "down",
]


def layer_kernel(sizes, names, *refs):
    nz, nk, ny, seqs, width = sizes
    r = types.SimpleNamespace(**dict(zip(names, refs, strict=True)))
    half = width // 2
    block = SLOTS * nk
    rows = nz * block
    groups = [range(g, min(g + GROUP, nz)) for g in range(0, nz, GROUP)]
    ep = lax.axis_index("ep")
    y = lax.axis_index("tp")
    z, k = ep // nk, ep % nk

    offsets = [offset % nz for offset in plane_offsets(nz)]

    def in_z(j):
        return ((z + offsets[j]) % nz) * nk + k, y

    def out_z(j):
        return ((z + (nz - offsets[j])) % nz) * nk + k, y

    def in_plane(q):
        return z * nk + (k + q) % nk, y

    def back_plane(q):
        return z * nk + (k + (nk - q)) % nk, y

    def in_y(q):
        return ep, (y + q) % ny

    def send(source, target, sends, receives, device):
        pltpu.make_async_remote_copy(
            src_ref=source,
            dst_ref=target,
            send_sem=sends,
            recv_sem=receives,
            device_id=device,
            device_id_type=MESH,
        ).start()

    def settle(ref, sem):
        pltpu.make_async_copy(ref, ref, sem).wait()

    barrier = pltpu.get_barrier_semaphore()
    peers = (
        [in_z(j) for j in range(nz - 1, 0, -1)]
        + [in_plane(q) for q in range(1, nk)]
        + [in_y(q) for q in range(1, ny)]
    )
    for device in peers:
        pl.semaphore_signal(barrier, inc=1, device_id=device, device_id_type=MESH)

    order = ["tokens", "low", "qkv", "up", "rows", "out", "gu", "down", "routes"]
    load_sem = {name: r.load_sem.at[i] for i, name in enumerate(order)}
    for s in range(0, seqs, 8):
        load_sem[s] = r.load_sem.at[len(order) + s // 8]

    def load(name, source, target):
        pltpu.make_async_copy(source, target, load_sem[name]).start()

    wide = r.recept.shape[1]
    low = r.decay_down.shape[0]
    heads = r.state.shape[1]
    head = wide // heads
    load("routes", r.routes, r.routes_vm)
    load("routes", r.weights, r.weights_vm)
    load("tokens", r.tokens, r.tokens_vm)
    load("low", r.decay_down, r.low_vm.at[pl.ds(0, low)])
    load("low", r.rate_down, r.low_vm.at[pl.ds(low, low)])
    load("qkv", r.recept, r.qkv_vm.at[:, pl.ds(0, wide)])
    load("qkv", r.key, r.qkv_vm.at[:, pl.ds(wide, wide)])
    load("qkv", r.value, r.qkv_vm.at[:, pl.ds(2 * wide, wide)])
    load("up", r.decay_up, r.up_vm.at[pl.ds(0, low), pl.ds(0, wide)])
    load("up", r.rate_up, r.up_vm.at[pl.ds(low, low), pl.ds(wide, wide)])
    load("rows", r.decay_base, r.base_vm)
    load("rows", r.rate_base, r.rate_vm)
    load("rows", r.gain, r.gain_vm)
    for s in range(0, seqs, 8):
        load(s, r.state.at[pl.ds(s, 8)], r.new_state.at[pl.ds(s, 8)])
    load("out", r.out_weight, r.out_vm)
    hidden = r.gate.shape[2]
    for q in range(ny):
        own = pl.ds(pl.multiple_of(((y + (ny - q)) % ny) * width, LANES), width)
        put = pl.ds(q * width, width)
        load("gu", r.gate.at[0, own, :], r.gu_vm.at[put, pl.ds(0, hidden)])
        load("gu", r.up.at[0, own, :], r.gu_vm.at[put, pl.ds(hidden, hidden)])
    for q in range(ny):
        ahead = pl.ds(pl.multiple_of(((y + q) % ny) * width, LANES), width)
        load("down", r.down.at[0, :, ahead], r.down_vm.at[:, pl.ds(q * width, width)])

    with scope("tables"):
        count = nk * nz
        row = lax.broadcasted_iota(I32, (count, seqs), 0)
        j_of, q_of = row % nz, row // nz
        away = jnp.zeros((count, seqs), I32)
        for j, offset in enumerate(offsets):
            away = jnp.where(j_of == j, offset, away)
        expert = ((z + away) % nz) * nk + (k + q_of) % nk
        member = jnp.zeros((count, seqs), F32)
        weight = jnp.zeros((count, seqs), F32)
        settle(r.routes_vm, load_sem["routes"])
        settle(r.weights_vm, load_sem["routes"])
        for c in range(r.routes.shape[0]):
            named = r.routes_vm[c : c + 1, :] == expert
            member = member + jnp.where(named, 1.0, 0.0)
            weight = weight + jnp.where(named, r.weights_vm[c : c + 1, :], 0.0)
        earlier_row = lax.broadcasted_iota(I32, (seqs, seqs), 0)
        later_row = lax.broadcasted_iota(I32, (seqs, seqs), 1)
        before = jnp.where(earlier_row < later_row, 1.0, 0.0).astype(BF16)
        earlier = dot(member.astype(BF16), before)
        code = jnp.where(member > 0.5, earlier, 9.0)
        r.info_out[...] = jnp.full(r.info_out.shape, 9.0, F32)
        for q in range(nk):
            r.info_out[q, 0:nz, 0:seqs] = code[q * nz : (q + 1) * nz]
            r.info_out[q, nz : 2 * nz, 0:seqs] = weight[q * nz : (q + 1) * nz]
        r.resid[:, seqs:, :] = jnp.zeros((nk, LANES - seqs, width), BF16)
        r.up_vm[0:low, wide:] = jnp.zeros((low, wide), BF16)
        r.up_vm[low:, 0:wide] = jnp.zeros((low, wide), BF16)

    with scope("project"):
        settle(r.tokens_vm, load_sem["tokens"])
        normed = row_norm(r.tokens_vm[...].astype(F32)).astype(BF16)
        settle(r.low_vm, load_sem["low"])
        lowered = dot_last(normed, r.low_vm[...])
        lane = lax.broadcasted_iota(I32, (seqs, 2 * low), 1)
        lowered = jnp.where(lane < low, jnp.tanh(lowered), lowered).astype(BF16)
        settle(r.qkv_vm, load_sem["qkv"])
        qkv = dot(normed, r.qkv_vm[...]).astype(BF16).astype(F32)
        recept, keys, values = qkv[:, :wide], qkv[:, wide : 2 * wide], qkv[:, 2 * wide :]
        settle(r.up_vm.at[pl.ds(0, low)], load_sem["up"])
        for ref in (r.base_vm, r.rate_vm, r.gain_vm):
            settle(ref, load_sem["rows"])
        raised = dot(lowered, r.up_vm[...])
        decay = jnp.exp(
            -jax.nn.sigmoid(raised[:, :wide] + r.base_vm[...]) * 0.6065306597126334
        )
        rate = jax.nn.sigmoid(raised[:, wide:] + r.rate_vm[...])

    lane = lax.broadcasted_iota(I32, (seqs, wide), 1)

    def head_sum(operand):
        total = jnp.zeros((seqs, wide), F32)
        for h in range(heads):
            mine = lane // head == h
            part = jnp.sum(jnp.where(mine, operand, 0.0), axis=1, keepdims=True)
            total = jnp.where(mine, part, total)
        return total

    with scope("heads"):
        unit = keys * lax.rsqrt(head_sum(keys * keys) + UNIT_EPS)
        unit_rate, key_rate = unit * rate, keys * rate

        def first_lanes(operand, h):
            return pltpu.roll(operand, wide - head * h, 1) if h else operand

        for h in range(heads):
            r.vec_vm[3 * h] = first_lanes(decay, h)
            r.vec_vm[3 * h + 1] = first_lanes(unit_rate, h)
            r.vec_vm[3 * h + 2] = first_lanes(key_rate, h)
        probes = [first_lanes(unit, h)[:, :head] for h in range(heads)]
        decayed = decay * recept
        probes += [first_lanes(decayed, h)[:, :head] for h in range(heads)]
        row8 = lax.broadcasted_iota(I32, (8, wide), 0)
        lane8 = lax.broadcasted_iota(I32, (8, wide), 1)
        found = [[], []]
        for s in range(0, seqs, 8):
            settle(r.new_state.at[pl.ds(s, 8)], load_sem[s])
            left = jnp.concatenate([probe[s : s + 8] for probe in probes], axis=0).astype(BF16)
            right = r.new_state[s : s + 8].reshape(8 * wide, head).astype(BF16)
            product = dot_last(left, right)
            for what in range(2):
                total = jnp.zeros((8, wide), F32)
                for h in range(heads):
                    at = (what * heads + h) * 8
                    for i in range(8):
                        here = jnp.logical_and(row8 == i, lane8 // head == h)
                        total = jnp.where(
                            here, product[at : at + 8, i * wide : (i + 1) * wide], total
                        )
                found[what].append(total)
        state_unit = jnp.concatenate(found[0], axis=0)
        head_out = (
            jnp.concatenate(found[1], axis=0)
            - state_unit * head_sum(unit_rate * recept)
            + values * head_sum(key_rate * recept)
        )
        r.col_vm[0] = state_unit
        r.col_vm[1] = values
        centred = head_out - head_sum(head_out) * (1.0 / head)
        spread = head_sum(centred * centred) * (1.0 / head)
        mixed = (centred * lax.rsqrt(spread + GROUP_EPS) * r.gain_vm[...]).astype(BF16)
        settle(r.out_vm, load_sem["out"])
        partial = dot(mixed, r.out_vm[...])
        for q in range(ny):
            r.part_out[q] = partial[:, q * width : (q + 1) * width].astype(BF16)

    with scope("barrier"):
        pl.semaphore_wait(barrier, len(peers))

    for q in range(1, ny):
        send(
            r.part_out.at[(y + q) % ny],
            r.part_in.at[q],
            r.part_send.at[0],
            r.part_recv.at[0],
            in_y(q),
        )
    for q in range(1, nk):
        send(r.info_out.at[q], r.info_in.at[q], r.info_send.at[0], r.info_recv.at[0], in_plane(q))

    with scope("reduce"):
        summed = r.part_out[y].astype(F32)
        settle(r.part_in.at[pl.ds(1, ny - 1)], r.part_recv.at[0])
        for q in range(1, ny):
            summed = summed + r.part_in[q].astype(F32)
        own = r.tokens_vm[:, pl.ds(pl.multiple_of(y * width, LANES), width)]
        r.resid[0, 0:seqs, :] = (own.astype(F32) + summed).astype(BF16)
    for q in range(1, nk):
        send(
            r.resid.at[0, pl.ds(0, seqs)],
            r.resid.at[q, pl.ds(0, seqs)],
            r.res_send.at[0],
            r.res_recv.at[0],
            in_plane(q),
        )

    with scope("pick"):
        rep_row = lax.broadcasted_iota(I32, (nz, SLOTS, nk, nz), 0).reshape(rows, nz)
        rep_col = lax.broadcasted_iota(I32, (nz, SLOTS, nk, nz), 3).reshape(rows, nz)
        repeat = jnp.where(rep_row == rep_col, 1.0, 0.0).astype(BF16)
        slot = lax.broadcasted_iota(I32, (nz, SLOTS, nk, LANES), 1).reshape(rows, LANES).astype(F32)
        source = lax.broadcasted_iota(I32, (nz, SLOTS, nk, LANES), 2).reshape(rows, LANES)
        settle(r.info_in.at[pl.ds(1, nk - 1)], r.info_recv.at[0])
        for q in range(nk):
            told = r.info_in if q else r.info_out
            spread = dot(repeat, told[q, 0:nz, :].astype(BF16))
            chosen = jnp.where(spread == slot, jnp.where(source == q, 1.0, 0.0), 0.0)
            r.pick[:, q * LANES : (q + 1) * LANES] = chosen.astype(BF16)

    with scope("gather"):
        settle(r.resid.at[pl.ds(1, nk - 1), pl.ds(0, seqs)], r.res_recv.at[0])
    with scope("dispatch"):
        outgoing = dot(r.pick[...], r.resid[...].reshape(nk * LANES, width))
        outgoing = outgoing.reshape(nz, block, width)
        r.z_out[...] = jnp.concatenate(
            [outgoing[:, :, :half], outgoing[:, :, half:]], axis=1
        ).astype(BF16)

    for j in send_order(nz):
        send(r.z_out.at[j], r.z_in.at[j], r.z_send.at[0], r.z_recv.at[j], in_z(j))

    def forward(j):
        held = r.z_in.at[j] if j else r.z_out.at[0]
        if j:
            settle(held, r.z_recv.at[j])
        for q in range(1, ny):
            send(held, r.y_in.at[q, j], r.y_send.at[0], r.y_recv.at[j // GROUP], in_y(q))

    def forward_group(group):
        for j in group:
            if j:
                forward(j)

    def load_experts(group):
        settle(r.gu_vm, load_sem["gu"])
        settle(r.down_vm, load_sem["down"])

    forward(0)

    def experts(group):
        at = (pl.ds(1, ny - 1), pl.ds(group[0], len(group)))
        settle(r.y_in.at[at], r.y_recv.at[group[0] // GROUP])
        columns = []
        for q in range(ny):
            pieces = []
            for j in group:
                if q:
                    held = r.y_in[q, j]
                elif j:
                    held = r.z_in[j]
                else:
                    held = r.z_out[0]
                held = held.astype(F32)
                pieces.append(jnp.concatenate([held[:block], held[block:]], axis=1))
            columns.append(jnp.concatenate(pieces, axis=0))
        features = jnp.concatenate(columns, axis=1)
        normed = row_norm(features).astype(BF16)
        pre = dot(normed, r.gu_vm[...])
        gated = jnp.minimum(pre[:, :hidden], CLAMP_LIMIT)
        linear = jnp.clip(pre[:, hidden:], -CLAMP_LIMIT, CLAMP_LIMIT)
        activated = (gated * jax.nn.sigmoid(GLU_ALPHA * gated) * (linear + 1.0)).astype(BF16)
        share = dot(activated, r.down_vm[...])
        for q in range(ny):
            for at, j in enumerate(group):
                piece = share[at * block : (at + 1) * block, q * width : (q + 1) * width]
                r.share_out[q, j] = jnp.concatenate(
                    [piece[:, :half], piece[:, half:]], axis=0
                ).astype(BF16)
        for j in group:
            for q in range(1, ny):
                send(
                    r.share_out.at[q, j],
                    r.share_in.at[q, j],
                    r.share_send.at[0],
                    r.share_recv.at[j // GROUP],
                    in_y(q),
                )

    def give_back(group):
        at = (pl.ds(1, ny - 1), pl.ds(group[0], len(group)))
        settle(r.share_in.at[at], r.share_recv.at[group[0] // GROUP])
        for j in group:
            total = r.share_out[0, j].astype(F32)
            for q in range(1, ny):
                total = total + r.share_in[q, j].astype(F32)
            total = total.astype(BF16)
            if j:
                r.back_out[j] = total
                send(
                    r.back_out.at[j], r.back_in.at[j], r.back_send.at[0], r.back_recv.at[0], out_z(j)
                )
            else:
                r.back_in[0] = total

    last = len(groups) - 1
    steps = []
    for g in range(last + 1):
        steps.append((forward_group, g))
        if g == last - 1:
            steps.append((load_experts, g))
            steps.append((experts, 0))
    for g in range(1 if last else 0, last + 1):
        steps.append((experts, g))
        if g >= 2:
            steps.append((give_back, g - 2))
    steps += [(give_back, g) for g in range(max(0, last - 1), last)]
    if not last:
        steps.insert(1, (load_experts, 0))
    for step, g in steps:
        with scope(f"{step.__name__}{g}"):
            step(groups[g])
    with scope("weights"):
        for q in range(nk):
            told = r.info_in if q else r.info_out
            weight = told[q, nz : 2 * nz, :]
            high = weight.astype(BF16)
            low_part = (weight - high.astype(F32)).astype(BF16)
            spread = dot(repeat, high) + dot(repeat, low_part)
            scaled = (spread * r.pick[:, q * LANES : (q + 1) * LANES].astype(F32)).T[0:seqs, :]
            high = scaled.astype(BF16)
            r.mix_hi[q] = high
            r.mix_lo[q] = (scaled - high.astype(F32)).astype(BF16)
    with scope("back_last"):
        give_back(groups[last])
    with scope("state"):
        for s in range(0, seqs, 8):
            lost = r.col_vm[0, s : s + 8, :].T
            gained = r.col_vm[1, s : s + 8, :].T
            for i in range(8):
                for h in range(heads):
                    at = pl.ds(s + i, 1)
                    span = slice(h * head, (h + 1) * head)
                    r.new_state[s + i, h] = (
                        r.new_state[s + i, h] * r.vec_vm[3 * h, at, :][:, :head]
                        - lost[span, i : i + 1] * r.vec_vm[3 * h + 1, at, :][:, :head]
                        + gained[span, i : i + 1] * r.vec_vm[3 * h + 2, at, :][:, :head]
                    )

    with scope("returned"):
        settle(r.back_in.at[pl.ds(1, nz - 1)], r.back_recv.at[0])
    with scope("mix"):
        returned = r.back_in[...].astype(F32)
        returned = jnp.concatenate([returned[:, :block], returned[:, block:]], axis=2)
        returned = returned.reshape(rows, width).astype(BF16)
        mixture = dot(r.mix_hi[...].reshape(nk * seqs, rows), returned) + dot(
            r.mix_lo[...].reshape(nk * seqs, rows), returned
        )
        r.mix_out[...] = mixture.reshape(nk, seqs, width).astype(BF16)
    for q in range(1, nk):
        send(r.mix_out.at[q], r.mix_in.at[q], r.mix_send.at[0], r.mix_recv.at[0], back_plane(q))
    with scope("final"):
        total = mixture[0:seqs]
        settle(r.mix_in.at[pl.ds(1, nk - 1)], r.mix_recv.at[0])
        for q in range(1, nk):
            total = total + r.mix_in[q].astype(F32)
        r.layer_out[...] = (r.resid[0, 0:seqs, :].astype(F32) + total).astype(BF16)
    with scope("drain"):
        settle(r.part_in.at[pl.ds(1, ny - 1)], r.part_send.at[0])
        settle(r.info_in.at[pl.ds(1, nk - 1)], r.info_send.at[0])
        settle(r.resid.at[pl.ds(1, nk - 1), pl.ds(0, seqs)], r.res_send.at[0])
        settle(r.z_in.at[pl.ds(1, nz - 1)], r.z_send.at[0])
        settle(r.y_in.at[pl.ds(1, ny - 1)], r.y_send.at[0])
        settle(r.share_in.at[pl.ds(1, ny - 1)], r.share_send.at[0])
        settle(r.back_in.at[pl.ds(1, nz - 1)], r.back_send.at[0])
        settle(r.mix_in.at[pl.ds(1, nk - 1)], r.mix_send.at[0])


def run_layer(sizes, *operands):
    nz, nk, ny, seqs, width = sizes
    args = dict(zip(INPUTS, operands, strict=True))
    rows = nz * SLOTS * nk
    message = (2 * SLOTS * nk, width // 2)
    hidden = args["gate"].shape[2]
    wide = args["recept"].shape[1]
    low = args["decay_down"].shape[0]
    state = args["state"].shape
    heads = state[1]
    dma = pltpu.SemaphoreType.DMA
    scratch = dict(
        tokens_vm=pltpu.VMEM((seqs, ny * width), BF16),
        qkv_vm=pltpu.VMEM((ny * width, 3 * wide), BF16),
        low_vm=pltpu.VMEM((2 * low, ny * width), BF16),
        up_vm=pltpu.VMEM((2 * low, 2 * wide), BF16),
        base_vm=pltpu.VMEM((1, wide), F32),
        rate_vm=pltpu.VMEM((1, wide), F32),
        gain_vm=pltpu.VMEM((1, wide), F32),
        routes_vm=pltpu.VMEM(args["routes"].shape, I32),
        weights_vm=pltpu.VMEM(args["weights"].shape, F32),
        vec_vm=pltpu.VMEM((3 * heads, seqs, wide), F32),
        col_vm=pltpu.VMEM((2, seqs, wide), F32),
        out_vm=pltpu.VMEM((wide, ny * width), BF16),
        gu_vm=pltpu.VMEM((ny * width, 2 * hidden), BF16),
        down_vm=pltpu.VMEM((hidden, ny * width), BF16),
        info_out=pltpu.VMEM((nk, 2 * nz, LANES), F32),
        info_in=pltpu.VMEM((nk, 2 * nz, LANES), F32),
        part_out=pltpu.VMEM((ny, seqs, width), BF16),
        part_in=pltpu.VMEM((ny, seqs, width), BF16),
        resid=pltpu.VMEM((nk, LANES, width), BF16),
        pick=pltpu.VMEM((rows, nk * LANES), BF16),
        mix_hi=pltpu.VMEM((nk, seqs, rows), BF16),
        mix_lo=pltpu.VMEM((nk, seqs, rows), BF16),
        z_out=pltpu.VMEM((nz, *message), BF16),
        z_in=pltpu.VMEM((nz, *message), BF16),
        y_in=pltpu.VMEM((ny, nz, *message), BF16),
        share_out=pltpu.VMEM((ny, nz, *message), BF16),
        share_in=pltpu.VMEM((ny, nz, *message), BF16),
        back_out=pltpu.VMEM((nz, *message), BF16),
        back_in=pltpu.VMEM((nz, *message), BF16),
        mix_out=pltpu.VMEM((nk, seqs, width), BF16),
        mix_in=pltpu.VMEM((nk, seqs, width), BF16),
        load_sem=dma((9 + seqs // 8,)),
    )
    waits = -(-nz // GROUP)
    for name, count in dict(
        info=1, part=1, res=1, z=nz, y=waits, share=waits, back=1, mix=1
    ).items():
        scratch[name + "_send"] = dma((1,))
        scratch[name + "_recv"] = dma((count,))
    hbm = pl.BlockSpec(memory_space=pltpu.HBM)
    vmem = pl.BlockSpec(memory_space=pltpu.VMEM)
    names = INPUTS + ["layer_out", "new_state"] + list(scratch)
    outs = ((seqs, width), BF16), (state, F32)
    results = pl.pallas_call(
        functools.partial(layer_kernel, sizes, names),
        out_shape=tuple(pltpu.VMEM(*out) for out in outs),
        in_specs=[hbm] * len(INPUTS),
        out_specs=(vmem, vmem),
        scratch_shapes=list(scratch.values()),
        compiler_params=pltpu.CompilerParams(
            collective_id=0, has_side_effects=True, vmem_limit_bytes=60 * 1024 * 1024
        ),
        name="layer",
    )(*operands)
    return pl.pallas_call(
        store_kernel,
        out_shape=tuple(jax.ShapeDtypeStruct(*out) for out in outs),
        in_specs=[vmem, vmem],
        out_specs=(hbm, hbm),
        scratch_shapes=[dma((PIECES + 1,))],
        compiler_params=pltpu.CompilerParams(vmem_limit_bytes=1024 * 1024),
        name="store",
    )(*results)


def store_kernel(layer_vm, state_vm, layer_ref, state_ref, sems):
    size = state_vm.shape[0] // PIECES
    copies = [pltpu.make_async_copy(layer_vm, layer_ref, sems.at[PIECES])]
    for i in range(PIECES):
        at = pl.ds(i * size, size)
        copies.append(pltpu.make_async_copy(state_vm.at[at], state_ref.at[at], sems.at[i]))
    for copy in copies:
        copy.start()
    for copy in copies:
        copy.wait()


def local(
    tokens,
    head_state,
    recept_weight,
    key_weight,
    value_weight,
    decay_down_factor,
    decay_up_factor,
    decay_base,
    rate_down_factor,
    rate_up_factor,
    rate_base,
    head_gain,
    out_weight,
    route_experts,
    route_weights,
    expert_gate,
    expert_up,
    expert_down,
):
    ny = lax.axis_size("tp")
    nz = lax.axis_size("ep") // PLANE
    seqs, model = tokens.shape

    return run_layer(
        (nz, PLANE, ny, seqs, model // ny),
        tokens,
        head_state,
        recept_weight,
        key_weight,
        value_weight,
        decay_down_factor.T,
        decay_up_factor,
        decay_base[None],
        rate_down_factor.T,
        rate_up_factor,
        rate_base[None],
        head_gain[None],
        out_weight,
        route_experts.T,
        route_weights.T,
        expert_gate,
        expert_up,
        expert_down,
    )


def solution(mesh):
    in_specs = (
        P("ep", None),
        P("ep", "tp", None, None),
        P(None, "tp"),
        P(None, "tp"),
        P(None, "tp"),
        P(),
        P(None, "tp"),
        P("tp"),
        P(),
        P(None, "tp"),
        P("tp"),
        P("tp"),
        P("tp", None),
        P("ep", None),
        P("ep", None),
        P("ep", None, "tp"),
        P("ep", None, "tp"),
        P("ep", "tp", None),
    )
    out_specs = (P("ep", "tp"), P("ep", "tp", None, None))
    return jax.shard_map(local, mesh=mesh, in_specs=in_specs, out_specs=out_specs, check_vma=False)
```

time: 138 us -> 64.9 us (0.47); the launches traced: 136 us -> 64.8 us
  blocking collectives: 69.5 us -> 0 us
  Pallas kernels: 0 us -> 64.2 us
  waiting for transfers between devices: 25.4 us -> 0 us
  starting transfers between devices: 15.3 us -> 0 us
  matrix products: 12 us -> 0 us
  local copies, waits for them, and re-layouts: 7.34 us -> 0 us
  other arithmetic: 5.73 us -> 0 us
    all_to_all x3 -> x0, blocking collectives: 69.5 us -> none  [the longest x1 41.9 us: local(): lax.all_to_all(buffer, 'ep', split_axis=0, concat_axis=0, tiled=True)]
    pallas_call x0 -> x2, Pallas kernels: none -> 64.2 us  [the longest x1 62.4 us: run_layer(): pl.pallas_call(functools.partial(layer_kernel, sizes, names), out_shape=t...]
    all_to_all x2 -> x0, waiting for transfers between devices: 25.4 us -> none  [the longest x1 20.2 us: local(): lax.all_to_all(shares, 'ep', split_axis=0, concat_axis=0, tiled=True)]
    all_to_all x2 -> x0, starting transfers between devices: 15.3 us -> none  [the longest x1 10.3 us: local(): lax.all_to_all(shares, 'ep', split_axis=0, concat_axis=0, tiled=True)]
    dot_general x11 -> x0, matrix products: 12 us -> none  [the longest x1 2.94 us: update_heads(): state_unit = jnp.einsum('shvk,shk->shv', head_state, unit_key)]
    reduce_sum x9 -> x0, other arithmetic: 2.26 us -> none  [the longest x2 1.21 us: row_norm(): jnp.mean(values * values, axis=-1, keepdims=True) + NORM_EPS]
    add x1 -> x0, other arithmetic: 2.07 us -> none  [update_heads(): head_state * decay_heads[:, :, None, :]]
    unnamed x24 -> x0, local copies, waits for them, and re-layouts: 2.05 us -> none
  transfers between devices with their start and end apart: 2 -> 0, of which waited for: 2 -> 0; matrix products, arithmetic and copies ran while one was open for 1% -> 0% of each run, Pallas kernels for 0% -> 0%
where the time goes in v2:
time: 64.9 us; the launch traced here: 64.8 us
  Pallas kernels  64.2 us (99%)
  between operations  0.65 us (1%)
    pallas_call x1, Pallas kernels, run_layer(): pl.pallas_call(functools.partial(layer_kernel, sizes, names), out_shape=t...  62.4 us
    pallas_call x1, Pallas kernels, run_layer(): pl.pallas_call(store_kernel, out_shape=tuple((jax.ShapeDtypeStruct(*out)...  1.73 us

profile of v2, /device:TPU:1, one launch (start us, length us, event | category | flops | bytes accessed | tf_op | source)
XLA Modules:
  0.0 64.8 jit_solution(15641089626877200725)
XLA Ops:
  0.6 62.4 %layer.1 = (bf16[48,256]{1,0:T(8,128)(2,1)S(1)}, f32[48,2,64,64]{3,2,1,0:T(8,128)S(1)}) custom-call(bf16[48,1024]{1,0:T(8,128)(2,1)} %refs_0_.1, f32[48,2,64,64]{3,2,1,0:T(8,128)} %refs_1_.1, bf16[1024,128]{1,0:T(8,128)(2,1)} %refs_2_.1, bf16[1024,128]{1,0:T(8,128)(2,1)} %refs_3_.1, bf16[1024,128]{1,0:T(8,128)(2,1)} %refs_4_.1, bf16[64,1024]{1,0:T(8,128)(2,1)} %bitcast.7, ...), custom_call_target="tpu_custom_call" | custom-call | tf_op jit(solution)/shard_map/layer/pallas_call | solution.py:532
  63.1 1.7 %store.1 = (bf16[48,256]{1,0:T(8,128)(2,1)}, f32[48,2,64,64]{3,2,1,0:T(8,128)}) custom-call(bf16[48,256]{1,0:T(8,128)(2,1)S(1)} %get-tuple-element.4.layer_vm, f32[48,2,64,64]{3,2,1,0:T(8,128)S(1)} %get-tuple-element.5.state_vm), custom_call_target="tpu_custom_call" | custom-call | tf_op jit(solution)/shard_map/store/pallas_call | solution.py:543

commit v3 on v2

--- a/solution.py
+++ b/solution.py
@@ -17,7 +17,10 @@
 PLANE = 8
 SLOTS = 3
 LANES = 128
-GROUP = 4
+WORK_ORDER = [0, 1, 2, 8, 7, 6, 5, 4, 3]
+SEND_ORDER = [1, 2, 8, 7, 6, 5, 4, 3]
+CUTS = [0, 3, 6, 10, 14, 16]
+PLAN = ["F0", "L", "W", "F1", "E0", "F2", "F3", "F4", "E1", "E2", "B0", "E3", "B1", "E4", "B2", "B3", "B4"]
 PIECES = 6
 SCOPES = False
 MESH = pl.DeviceIdType.MESH
@@ -25,20 +28,29 @@
 
 
 def plane_offsets(nz):
-    if nz == 16:
-        return [0, 1, -1, 2, -2, 3, -3, 8, 7, -7, 6, -6, 5, -5, 4, -4]
+    if nz == 2 * len(WORK_ORDER) - 2:
+        half = [way * d for d in WORK_ORDER for way in ((1, -1) if 0 < d < nz // 2 else (1,))]
+        return half
     return [0] + [way * d for d in range(1, nz // 2) for way in (1, -1)] + [nz // 2]
 
 
 def send_order(nz):
     offsets = plane_offsets(nz)
-    ranked = sorted(range(1, nz), key=lambda j: -abs(offsets[j]))
-    order = []
-    while ranked:
-        order.append(ranked.pop(0))
-        if ranked:
-            order.append(ranked.pop())
-    return order
+    if nz == 2 * len(SEND_ORDER):
+        return [j for d in SEND_ORDER for j in range(nz) if abs(offsets[j]) == d]
+    return list(range(1, nz))
+
+
+def plane_groups(nz):
+    cuts = CUTS if nz == 16 else [0, nz // 2, nz]
+    return [range(low, high) for low, high in zip(cuts, cuts[1:])]
+
+
+def plan(count):
+    if count == len(CUTS) - 1:
+        return PLAN
+    steps = ["F0", "L"] + [f"F{g}" for g in range(1, count)] + [f"E{g}" for g in range(count)]
+    return steps + [f"B{g}" for g in range(count)] + ["W"]
 
 
 def scope(name):
@@ -85,7 +97,8 @@
     half = width // 2
     block = SLOTS * nk
     rows = nz * block
-    groups = [range(g, min(g + GROUP, nz)) for g in range(0, nz, GROUP)]
+    groups = plane_groups(nz)
+    group_of = {j: g for g, group in enumerate(groups) for j in group}
     ep = lax.axis_index("ep")
     y = lax.axis_index("tp")
     z, k = ep // nk, ep % nk
@@ -106,6 +119,9 @@
 
     def in_y(q):
         return ep, (y + q) % ny
+
+    lanes = sorted(range(1, ny), key=lambda q: -min(q, ny - q))
+    others = sorted(range(1, nk), key=lambda q: -min(q, nk - q))
 
     def send(source, target, sends, receives, device):
         pltpu.make_async_remote_copy(
@@ -276,7 +292,7 @@
     with scope("barrier"):
         pl.semaphore_wait(barrier, len(peers))
 
-    for q in range(1, ny):
+    for q in lanes:
         send(
             r.part_out.at[(y + q) % ny],
             r.part_in.at[q],
@@ -284,7 +300,7 @@
             r.part_recv.at[0],
             in_y(q),
         )
-    for q in range(1, nk):
+    for q in others:
         send(r.info_out.at[q], r.info_in.at[q], r.info_send.at[0], r.info_recv.at[0], in_plane(q))
 
     with scope("reduce"):
@@ -294,7 +310,7 @@
             summed = summed + r.part_in[q].astype(F32)
         own = r.tokens_vm[:, pl.ds(pl.multiple_of(y * width, LANES), width)]
         r.resid[0, 0:seqs, :] = (own.astype(F32) + summed).astype(BF16)
-    for q in range(1, nk):
+    for q in others:
         send(
             r.resid.at[0, pl.ds(0, seqs)],
             r.resid.at[q, pl.ds(0, seqs)],
@@ -328,27 +344,24 @@
     for j in send_order(nz):
         send(r.z_out.at[j], r.z_in.at[j], r.z_send.at[0], r.z_recv.at[j], in_z(j))
 
-    def forward(j):
-        held = r.z_in.at[j] if j else r.z_out.at[0]
-        if j:
-            settle(held, r.z_recv.at[j])
-        for q in range(1, ny):
-            send(held, r.y_in.at[q, j], r.y_send.at[0], r.y_recv.at[j // GROUP], in_y(q))
+    def forward(source, group):
+        span = pl.ds(group[0], len(group))
+        for q in lanes:
+            target = r.y_in.at[q, span]
+            send(source.at[span], target, r.y_send.at[0], r.y_recv.at[group_of[group[0]]], in_y(q))
 
     def forward_group(group):
+        group = [j for j in group if j]
         for j in group:
-            if j:
-                forward(j)
-
-    def load_experts(group):
-        settle(r.gu_vm, load_sem["gu"])
-        settle(r.down_vm, load_sem["down"])
-
-    forward(0)
+            settle(r.z_in.at[j], r.z_recv.at[j])
+        if group:
+            forward(r.z_in, group)
+
+    forward(r.z_out, [0])
 
     def experts(group):
         at = (pl.ds(1, ny - 1), pl.ds(group[0], len(group)))
-        settle(r.y_in.at[at], r.y_recv.at[group[0] // GROUP])
+        settle(r.y_in.at[at], r.y_recv.at[group_of[group[0]]])
         columns = []
         for q in range(ny):
             pieces = []
@@ -375,19 +388,16 @@
                 r.share_out[q, j] = jnp.concatenate(
                     [piece[:, :half], piece[:, half:]], axis=0
                 ).astype(BF16)
-        for j in group:
-            for q in range(1, ny):
-                send(
-                    r.share_out.at[q, j],
-                    r.share_in.at[q, j],
-                    r.share_send.at[0],
-                    r.share_recv.at[j // GROUP],
-                    in_y(q),
-                )
+        for q in lanes:
+            at = (q, pl.ds(group[0], len(group)))
+            g = group_of[group[0]]
+            send(
+                r.share_out.at[at], r.share_in.at[at], r.share_send.at[0], r.share_recv.at[g], in_y(q)
+            )
 
     def give_back(group):
         at = (pl.ds(1, ny - 1), pl.ds(group[0], len(group)))
-        settle(r.share_in.at[at], r.share_recv.at[group[0] // GROUP])
+        settle(r.share_in.at[at], r.share_recv.at[group_of[group[0]]])
         for j in group:
             total = r.share_out[0, j].astype(F32)
             for q in range(1, ny):
@@ -401,24 +411,7 @@
             else:
                 r.back_in[0] = total
 
-    last = len(groups) - 1
-    steps = []
-    for g in range(last + 1):
-        steps.append((forward_group, g))
-        if g == last - 1:
-            steps.append((load_experts, g))
-            steps.append((experts, 0))
-    for g in range(1 if last else 0, last + 1):
-        steps.append((experts, g))
-        if g >= 2:
-            steps.append((give_back, g - 2))
-    steps += [(give_back, g) for g in range(max(0, last - 1), last)]
-    if not last:
-        steps.insert(1, (load_experts, 0))
-    for step, g in steps:
-        with scope(f"{step.__name__}{g}"):
-            step(groups[g])
-    with scope("weights"):
+    def return_weights():
         for q in range(nk):
             told = r.info_in if q else r.info_out
             weight = told[q, nz : 2 * nz, :]
@@ -429,8 +422,17 @@
             high = scaled.astype(BF16)
             r.mix_hi[q] = high
             r.mix_lo[q] = (scaled - high.astype(F32)).astype(BF16)
-    with scope("back_last"):
-        give_back(groups[last])
+
+    for step in plan(len(groups)):
+        with scope(step):
+            if step == "L":
+                settle(r.gu_vm, load_sem["gu"])
+                settle(r.down_vm, load_sem["down"])
+            elif step == "W":
+                return_weights()
+            else:
+                work = dict(F=forward_group, E=experts, B=give_back)[step[0]]
+                work(groups[int(step[1:])])
     with scope("state"):
         for s in range(0, seqs, 8):
             lost = r.col_vm[0, s : s + 8, :].T
@@ -455,7 +457,7 @@
             r.mix_lo[...].reshape(nk * seqs, rows), returned
         )
         r.mix_out[...] = mixture.reshape(nk, seqs, width).astype(BF16)
-    for q in range(1, nk):
+    for q in others:
         send(r.mix_out.at[q], r.mix_in.at[q], r.mix_send.at[0], r.mix_recv.at[0], back_plane(q))
     with scope("final"):
         total = mixture[0:seqs]
@@ -519,7 +521,7 @@
         mix_in=pltpu.VMEM((nk, seqs, width), BF16),
         load_sem=dma((9 + seqs // 8,)),
     )
-    waits = -(-nz // GROUP)
+    waits = len(plane_groups(nz))
     for name, count in dict(
         info=1, part=1, res=1, z=nz, y=waits, share=waits, back=1, mix=1
     ).items():

time: 64.9 us -> 64.1 us (0.988)
  Pallas kernels: 64.2 us -> 63.4 us
    pallas_call x1, Pallas kernels: 62.4 us -> 61.6 us  [run_layer(): pl.pallas_call(functools.partial(layer_kernel, sizes, names), out_shape=t...]
where the time goes in v3:
time: 64.1 us; the launch traced here: 64 us
  Pallas kernels  63.4 us (99%)
  between operations  0.65 us (1%)
    pallas_call x1, Pallas kernels, run_layer(): pl.pallas_call(functools.partial(layer_kernel, sizes, names), out_shape=t...  61.6 us
    pallas_call x1, Pallas kernels, run_layer(): pl.pallas_call(store_kernel, out_shape=tuple((jax.ShapeDtypeStruct(*out)...  1.73 us

profile of v3, /device:TPU:1, one launch (start us, length us, event | category | flops | bytes accessed | tf_op | source)
XLA Modules:
  0.0 64.0 jit_solution(14922322557145665806)
XLA Ops:
  0.6 61.6 %layer.1 = (bf16[48,256]{1,0:T(8,128)(2,1)S(1)}, f32[48,2,64,64]{3,2,1,0:T(8,128)S(1)}) custom-call(bf16[48,1024]{1,0:T(8,128)(2,1)} %refs_0_.1, f32[48,2,64,64]{3,2,1,0:T(8,128)} %refs_1_.1, bf16[1024,128]{1,0:T(8,128)(2,1)} %refs_2_.1, bf16[1024,128]{1,0:T(8,128)(2,1)} %refs_3_.1, bf16[1024,128]{1,0:T(8,128)(2,1)} %refs_4_.1, bf16[64,1024]{1,0:T(8,128)(2,1)} %bitcast.7, ...), custom_call_target="tpu_custom_call" | custom-call | tf_op jit(solution)/shard_map/layer/pallas_call | solution.py:534
  62.3 1.7 %store.1 = (bf16[48,256]{1,0:T(8,128)(2,1)}, f32[48,2,64,64]{3,2,1,0:T(8,128)}) custom-call(bf16[48,256]{1,0:T(8,128)(2,1)S(1)} %get-tuple-element.4.layer_vm, f32[48,2,64,64]{3,2,1,0:T(8,128)S(1)} %get-tuple-element.5.state_vm), custom_call_target="tpu_custom_call" | custom-call | tf_op jit(solution)/shard_map/store/pallas_call | solution.py:545

commit v4 on v3

--- a/solution.py
+++ b/solution.py
@@ -19,8 +19,8 @@
 LANES = 128
 WORK_ORDER = [0, 1, 2, 8, 7, 6, 5, 4, 3]
 SEND_ORDER = [1, 2, 8, 7, 6, 5, 4, 3]
-CUTS = [0, 3, 6, 10, 14, 16]
-PLAN = ["F0", "L", "W", "F1", "E0", "F2", "F3", "F4", "E1", "E2", "B0", "E3", "B1", "E4", "B2", "B3", "B4"]
+CUTS = [0, 3, 5, 9, 13, 16]
+PLAN = ["F0", "L", "F1", "W", "E0", "E1", "F2", "F3", "F4", "B0", "B1", "E2", "E3", "E4", "B2", "B3", "B4"]
 PIECES = 6
 SCOPES = False
 MESH = pl.DeviceIdType.MESH

time: 64.1 us -> 63.2 us (0.986)
  Pallas kernels: 63.4 us -> 62.5 us
    pallas_call x1, Pallas kernels: 61.6 us -> 60.8 us  [run_layer(): pl.pallas_call(functools.partial(layer_kernel, sizes, names), out_shape=t...]
where the time goes in v4:
time: 63.2 us; the launch traced here: 63.1 us
  Pallas kernels  62.5 us (99%)
  between operations  0.65 us (1%)
    pallas_call x1, Pallas kernels, run_layer(): pl.pallas_call(functools.partial(layer_kernel, sizes, names), out_shape=t...  60.8 us
    pallas_call x1, Pallas kernels, run_layer(): pl.pallas_call(store_kernel, out_shape=tuple((jax.ShapeDtypeStruct(*out)...  1.73 us

profile of v4, /device:TPU:1, one launch (start us, length us, event | category | flops | bytes accessed | tf_op | source)
XLA Modules:
  0.0 63.1 jit_solution(13559571563277320669)
XLA Ops:
  0.6 60.8 %layer.1 = (bf16[48,256]{1,0:T(8,128)(2,1)S(1)}, f32[48,2,64,64]{3,2,1,0:T(8,128)S(1)}) custom-call(bf16[48,1024]{1,0:T(8,128)(2,1)} %refs_0_.1, f32[48,2,64,64]{3,2,1,0:T(8,128)} %refs_1_.1, bf16[1024,128]{1,0:T(8,128)(2,1)} %refs_2_.1, bf16[1024,128]{1,0:T(8,128)(2,1)} %refs_3_.1, bf16[1024,128]{1,0:T(8,128)(2,1)} %refs_4_.1, bf16[64,1024]{1,0:T(8,128)(2,1)} %bitcast.7, ...), custom_call_target="tpu_custom_call" | custom-call | tf_op jit(solution)/shard_map/layer/pallas_call | solution.py:534
  61.4 1.7 %store.1 = (bf16[48,256]{1,0:T(8,128)(2,1)}, f32[48,2,64,64]{3,2,1,0:T(8,128)}) custom-call(bf16[48,256]{1,0:T(8,128)(2,1)S(1)} %get-tuple-element.4.layer_vm, f32[48,2,64,64]{3,2,1,0:T(8,128)S(1)} %get-tuple-element.5.state_vm), custom_call_target="tpu_custom_call" | custom-call | tf_op jit(solution)/shard_map/store/pallas_call | solution.py:545

commit v5 on v4

--- a/solution.py
+++ b/solution.py
@@ -334,15 +334,21 @@
 
     with scope("gather"):
         settle(r.resid.at[pl.ds(1, nk - 1), pl.ds(0, seqs)], r.res_recv.at[0])
-    with scope("dispatch"):
-        outgoing = dot(r.pick[...], r.resid[...].reshape(nk * LANES, width))
-        outgoing = outgoing.reshape(nz, block, width)
-        r.z_out[...] = jnp.concatenate(
+    def dispatch(low, high):
+        outgoing = dot(
+            r.pick[low * block : high * block, :], r.resid[...].reshape(nk * LANES, width)
+        ).reshape(high - low, block, width)
+        r.z_out[low:high] = jnp.concatenate(
             [outgoing[:, :, :half], outgoing[:, :, half:]], axis=1
         ).astype(BF16)
-
-    for j in send_order(nz):
-        send(r.z_out.at[j], r.z_in.at[j], r.z_send.at[0], r.z_recv.at[j], in_z(j))
+        for j in send_order(nz):
+            if low <= j < high:
+                send(r.z_out.at[j], r.z_in.at[j], r.z_send.at[0], r.z_recv.at[j], in_z(j))
+
+    with scope("dispatch"):
+        cut = 6 if nz == 16 else nz // 2
+        dispatch(0, cut)
+        dispatch(cut, nz)
 
     def forward(source, group):
         span = pl.ds(group[0], len(group))

time: 63.2 us -> 63.7 us (level)
  no operation moved by 1% of the time
where the time goes in v5:
time: 63.7 us; the launch traced here: 63.6 us
  Pallas kernels  62.9 us (99%)
  between operations  0.65 us (1%)
    pallas_call x1, Pallas kernels, run_layer(): pl.pallas_call(functools.partial(layer_kernel, sizes, names), out_shape=t...  61.2 us
    pallas_call x1, Pallas kernels, run_layer(): pl.pallas_call(store_kernel, out_shape=tuple((jax.ShapeDtypeStruct(*out)...  1.73 us

profile of v5, /device:TPU:1, one launch (start us, length us, event | category | flops | bytes accessed | tf_op | source)
XLA Modules:
  0.0 63.6 jit_solution(8416240146634922902)
XLA Ops:
  0.6 61.2 %layer.1 = (bf16[48,256]{1,0:T(8,128)(2,1)S(1)}, f32[48,2,64,64]{3,2,1,0:T(8,128)S(1)}) custom-call(bf16[48,1024]{1,0:T(8,128)(2,1)} %refs_0_.1, f32[48,2,64,64]{3,2,1,0:T(8,128)} %refs_1_.1, bf16[1024,128]{1,0:T(8,128)(2,1)} %refs_2_.1, bf16[1024,128]{1,0:T(8,128)(2,1)} %refs_3_.1, bf16[1024,128]{1,0:T(8,128)(2,1)} %refs_4_.1, bf16[64,1024]{1,0:T(8,128)(2,1)} %bitcast.7, ...), custom_call_target="tpu_custom_call" | custom-call | tf_op jit(solution)/shard_map/layer/pallas_call | solution.py:540
  61.8 1.7 %store.1 = (bf16[48,256]{1,0:T(8,128)(2,1)}, f32[48,2,64,64]{3,2,1,0:T(8,128)}) custom-call(bf16[48,256]{1,0:T(8,128)(2,1)S(1)} %get-tuple-element.4.layer_vm, f32[48,2,64,64]{3,2,1,0:T(8,128)S(1)} %get-tuple-element.5.state_vm), custom_call_target="tpu_custom_call" | custom-call | tf_op jit(solution)/shard_map/store/pallas_call | solution.py:551
